TPU v7x, 1024 devices: a whole 8x8x8 slice. The times are simulated.
1024 devices in a mesh: ep: 64 (over z, y), tp: 16 (over x, core).
Axes of the slice: x: 8, y: 8, z: 8, core: 2. Of those that a mesh axis runs over, the one named last changes fastest.
Arguments:
- tokens: bfloat16 [8192, 2048], P('ep'), may hold values from -6 to 6
- cotangent: bfloat16 [8192, 2048], P('ep'), may hold values from -0.796875 to 0.796875
- mix_weights: bfloat16 [8192, 2], P('ep'), may hold values from 0.049804688 to 1
- routes: int32 [8192, 2], P('ep'), may hold values from 0 to 63, all different within a row; in each aligned block of 128 rows (0 to 127, 128 to 255, ...) at most 5 rows name the same one
- gate_proj: bfloat16 [64, 2048, 2048], P('ep', None, 'tp'), may hold values from -0.125 to 0.125
- up_proj: bfloat16 [64, 2048, 2048], P('ep', None, 'tp'), may hold values from -0.125 to 0.125
- down_proj: bfloat16 [64, 2048, 2048], P('ep', 'tp'), may hold values from -0.125 to 0.125
Outputs:
- token_grad: bfloat16 [8192, 2048], P('ep', 'tp')
- mix_grad: bfloat16 [8192, 2], P('ep')
- gate_grad: bfloat16 [64, 2048, 2048], P('ep', None, 'tp')
- up_grad: bfloat16 [64, 2048, 2048], P('ep', None, 'tp')
- down_grad: bfloat16 [64, 2048, 2048], P('ep', 'tp')
Inputs may be any that keep to these rules, and one draw needn't show every extreme that they name: `routes`: each row names 2 different experts; in each aligned block of 128 rows (the rows of one device) no expert is named more than 5 times, a bound that some block reaches.
All inputs are finite; a program needn't handle non-finite values.
Results may differ from a plain program's by a relative error of at most 0.018.
Values may be sent and summed in bfloat16 or wider, within the bound.
A program may use at most 128 MiB of HBM per device.

v0:
```python
import math

import jax
import jax.numpy as jnp
from jax import lax
from jax.sharding import PartitionSpec as P


def sent_together(arrays, axis, split_dim, concat_dim, along):
    widths = [math.prod(a.shape[along:]) for a in arrays]
    both = jnp.concatenate(
        [a.reshape(*a.shape[:along], w) for a, w in zip(arrays, widths)], axis=along
    )
    whole = lax.all_to_all(both, axis, split_axis=split_dim, concat_axis=concat_dim, tiled=True)
    pieces = jnp.split(whole, [sum(widths[:k]) for k in range(1, len(widths))], axis=along)
    return tuple(
        (b.reshape(*whole.shape[:along], *a.shape[along:]) for a, b in zip(arrays, pieces))
    )


def laid_out(pieces, dim):
    dims = list(pieces.shape[1:])
    dims[dim] *= pieces.shape[0]
    return jnp.moveaxis(pieces, 0, dim).reshape(dims)


def from_everyone(value, axis):
    copies = jnp.broadcast_to(value, (lax.axis_size(axis), *value.shape))
    return lax.all_to_all(copies, axis, split_axis=0, concat_axis=0, tiled=True)


def gathered_copies(value, axis, dim):
    return laid_out(from_everyone(value, axis), dim)


def in_one_piece(arrays, axis, dim, along):
    both = jnp.concatenate(arrays, axis=along)
    whole, at, done = (gathered_copies(both, axis, dim), 0, [])
    for a in arrays:
        done.append(lax.slice_in_dim(whole, at, at + a.shape[along], axis=along))
        at += a.shape[along]
    return tuple(done)


def over_copies(value, axis):
    return from_everyone(value, axis).sum(axis=0)


def cut_along(value, dim, devices):
    before, after = (value.shape[:dim], value.shape[dim + 1 :])
    return jnp.moveaxis(value.reshape(*before, devices, -1, *after), dim, 0)


def sent_and_summed(value, axis, dim):
    devices = lax.axis_size(axis)
    pieces = lax.all_to_all(cut_along(value, dim, devices), axis, 0, 0, tiled=True)
    return jnp.sum(pieces.astype(jnp.float32), axis=0)


def silu_slope(pre):
    sig = jax.nn.sigmoid(pre)
    return sig * (1.0 + pre * (1.0 - sig))


def place_rows(source, target, owner, experts, slots):
    filled = (
        jnp.zeros((experts * slots, source.shape[1]), source.dtype).at[target].set(source[owner])
    )
    return filled.reshape(experts, slots, source.shape[1])


def on_device(tokens, cotangent, mix_weights, routes, gate_proj, up_proj, down_proj):
    experts = lax.axis_size("ep")
    lanes = lax.axis_size("tp")
    tok_rows, width = tokens.shape
    top = routes.shape[1]
    slots = 5 * tok_rows * top // (4 * experts)
    flat = routes.reshape(-1)
    onehot = (flat[:, None] == jnp.arange(experts, dtype=jnp.int32)[None, :]).astype(jnp.int32)
    before = jnp.cumsum(onehot, axis=0) - onehot
    rank = jnp.sum(before * onehot, axis=1)
    target = flat * slots + rank
    owner = jnp.arange(tok_rows * top, dtype=jnp.int32) // top
    mix_slots = (
        jnp.zeros((experts * slots,), jnp.bfloat16)
        .at[target]
        .set(mix_weights.reshape(-1))
        .reshape(experts, slots)
    )
    share = width // lanes
    start = lax.axis_index("tp") * share
    token_part = lax.dynamic_slice_in_dim(tokens, start, share, 1)
    back_part = lax.dynamic_slice_in_dim(cotangent, start, share, 1)
    row_part, grad_part, mix_in = sent_together(
        (
            place_rows(token_part, target, owner, experts, slots),
            place_rows(back_part, target, owner, experts, slots),
            mix_slots,
        ),
        "ep",
        0,
        0,
        2,
    )
    rows, backs = in_one_piece((row_part, grad_part), "tp", 2, 0)
    count = experts * slots
    rows = rows.reshape(count, width)
    backs = backs.reshape(count, width)
    weight = mix_in.reshape(count, 1).astype(jnp.float32)
    gate_w = gate_proj[0]
    up_w = up_proj[0]
    down_w = down_proj[0]
    pre_gate = jnp.dot(rows, gate_w, preferred_element_type=jnp.float32)
    pre_up = jnp.dot(rows, up_w, preferred_element_type=jnp.float32)
    active = jax.nn.silu(pre_gate)
    hidden = (active * pre_up).astype(jnp.bfloat16)
    back_hidden = lax.dot_general(
        backs, down_w, (((1,), (1,)), ((), ())), preferred_element_type=jnp.float32
    )
    mix_part = jnp.sum(hidden.astype(jnp.float32) * back_hidden, axis=1).reshape(experts, slots)
    pair_mix = over_copies(mix_part, "tp").astype(jnp.bfloat16)
    weighted = (weight * hidden.astype(jnp.float32)).astype(jnp.bfloat16)
    down_grad = lax.dot_general(
        weighted, backs, (((0,), (0,)), ((), ())), preferred_element_type=jnp.float32
    ).astype(jnp.bfloat16)
    scaled = weight * back_hidden
    back_gate = (scaled * pre_up * silu_slope(pre_gate)).astype(jnp.bfloat16)
    back_up = (scaled * active).astype(jnp.bfloat16)
    gate_grad = lax.dot_general(
        rows, back_gate, (((0,), (0,)), ((), ())), preferred_element_type=jnp.float32
    ).astype(jnp.bfloat16)
    up_grad = lax.dot_general(
        rows, back_up, (((0,), (0,)), ((), ())), preferred_element_type=jnp.float32
    ).astype(jnp.bfloat16)
    partial_value = lax.dot_general(
        back_gate, gate_w, (((1,), (1,)), ((), ())), preferred_element_type=jnp.float32
    )
    partial_value = partial_value + lax.dot_general(
        back_up, up_w, (((1,), (1,)), ((), ())), preferred_element_type=jnp.float32
    )
    partial_value = partial_value.astype(jnp.bfloat16).astype(jnp.float32)
    pair_grad = sent_and_summed(
        partial_value.reshape(experts, slots, width).astype(jnp.bfloat16), "tp", 2
    ).astype(jnp.bfloat16)
    grad_back, mix_back = sent_together((pair_grad, pair_mix), "ep", 0, 0, 2)
    columns = grad_back.shape[2]
    picked = grad_back.reshape(count, columns)[target].astype(jnp.float32)
    token_grad = jnp.sum(picked.reshape(tok_rows, top, columns), axis=1).astype(jnp.bfloat16)
    mix_grad = mix_back.reshape(count)[target].reshape(tok_rows, top)
    return (token_grad, mix_grad, gate_grad[None], up_grad[None], down_grad[None])


def solution(mesh):
    in_specs = (
        P("ep", None),
        P("ep", None),
        P("ep", None),
        P("ep", None),
        P("ep", None, "tp"),
        P("ep", None, "tp"),
        P("ep", "tp", None),
    )
    out_specs = (
        P("ep", "tp"),
        P("ep", None),
        P("ep", None, "tp"),
        P("ep", None, "tp"),
        P("ep", "tp", None),
    )
    return jax.shard_map(
        on_device, mesh=mesh, in_specs=in_specs, out_specs=out_specs, check_vma=False
    )
```

profile of v0, /device:TPU:1, one launch (start us, length us, event | category | flops | bytes accessed | tf_op | source)
XLA Modules:
  0.0 203.6 jit_solution(4394051726563113514)
XLA Ops:
  0.7 0.8 copy.53
  1.8 0.7 broadcast_multiply_fusion
  3.7 0.8 constant_dynamic-slice_fusion
  4.5 1.8 scatter_custom_fusion
  6.4 1.8 scatter_custom_fusion.1
  8.5 2.2 %scatter_custom_fusion.2 = bf16[320]{0:T(512)(128)(2,1)S(1)} fusion(s32[256]{0:T(256)S(1)} %bitcast.96, bf16[256]{0:T(256)(128)(2,1)S(1)} %reshape.214, bf16[]{:T(256)} %constant.20.clone.1), kind=kCustom, calls=%fused_computation.77 | custom fusion | bytes 642 | tf_op jit(solution)/shard_map/scatter | solution.py:87
  11.0 38.8 %all_to_all.25 = bf16[64,5,257]{2,1,0:T(8,128)(2,1)S(1)} all-to-all(bf16[64,5,257]{2,1,0:T(8,128)(2,1)S(1)} %pad_maximum_fusion), channel_id=1, replica_groups=mesh['ep'=64,'tp'=16] {'ep'}, dimensions={0} | all-to-all | bytes 328960 | tf_op jit(solution)/shard_map/all_to_all | solution.py:14
  50.0 2.1 %broadcast_in_dim.13 = bf16[16,128,5,128]{3,1,2,0:T(8,128)(2,1)} broadcast(bf16[128,5,128]{2,0,1:T(8,128)(2,1)S(1)} %copy.58), dimensions={1,2,3} | broadcast | bytes 2785280 | tf_op jit(solution)/shard_map/broadcast_in_dim | solution.py:28
  52.1 10.0 %all-to-all-start.1 = ((bf16[16,128,5,128]{3,1,2,0:T(8,128)(2,1)}), bf16[16,128,5,128]{3,1,2,0:T(8,128)(2,1)S(1)}, u32[]{:S(2)}, u32[]{:S(2)}) async-start(bf16[16,128,5,128]{3,1,2,0:T(8,128)(2,1)} %broadcast_in_dim.13), calls=%async_computation.1 | async-start | bytes 5242880 | tf_op jit(solution)/shard_map/all_to_all | solution.py:29
  62.1 0.8 convert_reduce_fusion
  62.9 0.9 reshape.161
  63.8 57.9 %all-to-all-done.1 = bf16[16,128,5,128]{3,1,2,0:T(8,128)(2,1)S(1)} async-done(((bf16[16,128,5,128]{3,1,2,0:T(8,128)(2,1)}), bf16[16,128,5,128]{3,1,2,0:T(8,128)(2,1)S(1)}, u32[]{:S(2)}, u32[]{:S(2)}) %all-to-all-start.1) | async-done | bytes 2621472 | tf_op jit(solution)/shard_map/all_to_all | solution.py:29
  122.3 0.8 copy.60
  123.7 0.9 copy-done.5
  125.1 0.8 copy.59
  127.7 0.7 reshape.235
  128.5 5.5 %all-to-all-start.3 = ((f32[16,1,320]{2,1,0:T(1,128)}), f32[16,1,320]{2,1,0:T(1,128)S(1)}, u32[]{:S(2)}, u32[]{:S(2)}) async-start(f32[16,1,320]{2,1,0:T(1,128)} %reshape.235), calls=%async_computation.3 | async-start | bytes 49152 | tf_op jit(solution)/shard_map/all_to_all | solution.py:29
  134.0 1.5 fusion.4
  135.9 1.4 copy.99
  137.3 4.1 %all-to-all-done.3 = f32[16,1,320]{2,1,0:T(1,128)S(1)} async-done(((f32[16,1,320]{2,1,0:T(1,128)}), f32[16,1,320]{2,1,0:T(1,128)S(1)}, u32[]{:S(2)}, u32[]{:S(2)}) %all-to-all-start.3) | async-done | bytes 20512 | tf_op jit(solution)/shard_map/all_to_all | solution.py:29
  141.4 4.0 %all-to-all-start.2 = ((bf16[16,64,5,128]{3,1,2,0:T(8,128)(2,1)}), bf16[16,64,5,128]{3,1,2,0:T(8,128)(2,1)S(1)}, u32[]{:S(2)}, u32[]{:S(2)}) async-start(bf16[16,64,5,128]{3,1,2,0:T(8,128)(2,1)} %bitcast.82), calls=%async_computation.2 | async-start | bytes 2621440 | tf_op jit(solution)/shard_map/all_to_all | solution.py:56
  145.4 1.5 fusion.2
  146.9 1.5 fusion.1
  148.9 0.7 reduce.8
  149.9 28.8 %all-to-all-done.2 = bf16[16,64,5,128]{3,1,2,0:T(8,128)(2,1)S(1)} async-done(((bf16[16,64,5,128]{3,1,2,0:T(8,128)(2,1)}), bf16[16,64,5,128]{3,1,2,0:T(8,128)(2,1)S(1)}, u32[]{:S(2)}, u32[]{:S(2)}) %all-to-all-start.2) | async-done | bytes 1310752 | tf_op jit(solution)/shard_map/all_to_all | solution.py:56
  179.0 0.8 pad_maximum_fusion.2
  179.8 4.6 %all-to-all-start.4 = ((bf16[64,5,129]{2,1,0:T(8,128)(2,1)}), bf16[64,5,129]{2,1,0:T(8,128)(2,1)S(1)}, u32[]{:S(2)}, u32[]{:S(2)}) async-start(bf16[64,5,129]{2,1,0:T(8,128)(2,1)} %pad_maximum_fusion.2), calls=%async_computation.4 | async-start | bytes 524288 | tf_op jit(solution)/shard_map/all_to_all | solution.py:14
  184.4 1.4 fusion.3
  185.8 13.1 %all-to-all-done.4 = bf16[64,5,129]{2,1,0:T(8,128)(2,1)S(1)} async-done(((bf16[64,5,129]{2,1,0:T(8,128)(2,1)}), bf16[64,5,129]{2,1,0:T(8,128)(2,1)S(1)}, u32[]{:S(2)}, u32[]{:S(2)}) %all-to-all-start.4) | async-done | bytes 82592 | tf_op jit(solution)/shard_map/all_to_all | solution.py:14
  199.2 1.9 gather_fusion.1
  202.0 0.9 gather_fusion
  202.9 0.8 reduce_sum.58
  (59 shorter events, 8.2 us)
Async XLA Ops:
  0.6 122.5 %copy-start = (bf16[1,2048,128]{2,1,0:T(8,128)(2,1)S(1)}, bf16[1,2048,128]{2,1,0:T(8,128)(2,1)}, u32[]{:S(2)}) copy-start(bf16[1,2048,128]{2,1,0:T(8,128)(2,1)} %param.11) | copy-start | bytes 1572868
  0.6 7.6 %copy-start.6 = (bf16[128,2]{0,1:T(2,128)(2,1)S(1)}, bf16[128,2]{0,1:T(2,128)(2,1)}, u32[]{:S(2)}) copy-start(bf16[128,2]{0,1:T(2,128)(2,1)} %param.9) | copy-start | bytes 1540
  52.1 69.6 %all-to-all-start.1 = ((bf16[16,128,5,128]{3,1,2,0:T(8,128)(2,1)}), bf16[16,128,5,128]{3,1,2,0:T(8,128)(2,1)S(1)}, u32[]{:S(2)}, u32[]{:S(2)}) async-start(bf16[16,128,5,128]{3,1,2,0:T(8,128)(2,1)} %broadcast_in_dim.13), calls=%async_computation.1 | async-start | bytes 5242880 | tf_op jit(solution)/shard_map/all_to_all | solution.py:29
  123.1 1.9 copy-start.3
  123.1 1.4 copy-start.5
  125.1 1.0 copy-start.7
  126.0 1.1 copy-start.1
  128.5 12.9 %all-to-all-start.3 = ((f32[16,1,320]{2,1,0:T(1,128)}), f32[16,1,320]{2,1,0:T(1,128)S(1)}, u32[]{:S(2)}, u32[]{:S(2)}) async-start(f32[16,1,320]{2,1,0:T(1,128)} %reshape.235), calls=%async_computation.3 | async-start | bytes 49152 | tf_op jit(solution)/shard_map/all_to_all | solution.py:29
  141.4 4.0 %copy-start.4 = (bf16[64,5,16,128]{3,2,1,0:T(8,128)(2,1)S(1)}, bf16[64,5,16,128]{3,2,1,0:T(8,128)(2,1)}, u32[]{:S(2)}) copy-start(bf16[64,5,16,128]{3,2,1,0:T(8,128)(2,1)} %copy-done.3) | copy-start | bytes 3932164
  141.4 37.3 %all-to-all-start.2 = ((bf16[16,64,5,128]{3,1,2,0:T(8,128)(2,1)}), bf16[16,64,5,128]{3,1,2,0:T(8,128)(2,1)S(1)}, u32[]{:S(2)}, u32[]{:S(2)}) async-start(bf16[16,64,5,128]{3,1,2,0:T(8,128)(2,1)} %bitcast.82), calls=%async_computation.2 | async-start | bytes 2621440 | tf_op jit(solution)/shard_map/all_to_all | solution.py:56
  149.9 34.6 %copy-start.2 = (bf16[64,5,16,128]{3,2,1,0:T(8,128)(2,1)S(1)}, bf16[64,5,16,128]{3,2,1,0:T(8,128)(2,1)}, u32[]{:S(2)}) copy-start(bf16[64,5,16,128]{3,2,1,0:T(8,128)(2,1)} %copy-done.1) | copy-start | bytes 3932164
  179.8 19.1 %all-to-all-start.4 = ((bf16[64,5,129]{2,1,0:T(8,128)(2,1)}), bf16[64,5,129]{2,1,0:T(8,128)(2,1)S(1)}, u32[]{:S(2)}, u32[]{:S(2)}) async-start(bf16[64,5,129]{2,1,0:T(8,128)(2,1)} %pad_maximum_fusion.2), calls=%async_computation.4 | async-start | bytes 524288 | tf_op jit(solution)/shard_map/all_to_all | solution.py:14
where the time goes:
time: 204 us
  waiting for transfers between devices  104 us (51%)
  blocking collectives  38.8 us (19%)
  starting transfers between devices  24.2 us (12%)
  local copies, waits for them, and re-layouts  22.8 us (11%)
  matrix products  7.98 us (4%)
  other arithmetic  4.91 us (2%)
    all_to_all x2, waiting for transfers between devices, from_everyone(): return lax.all_to_all(copies, axis, split_axis=0, concat_axis=0, tiled=True)  62 us
    all_to_all x1, blocking collectives, sent_together(): lax.all_to_all(both, axis, split_axis=split_dim, concat_axis=concat_dim,...  38.8 us
    all_to_all x1, waiting for transfers between devices, sent_and_summed(): lax.all_to_all(cut_along(value, dim, devices), axis, 0, 0, tiled=True)  28.8 us
    all_to_all x2, starting transfers between devices, from_everyone(): return lax.all_to_all(copies, axis, split_axis=0, concat_axis=0, tiled=True)  15.6 us
    all_to_all x1, waiting for transfers between devices, sent_together(): lax.all_to_all(both, axis, split_axis=split_dim, concat_axis=concat_dim,...  13.1 us
    all_to_all x1, starting transfers between devices, sent_together(): lax.all_to_all(both, axis, split_axis=split_dim, concat_axis=concat_dim,...  4.61 us
    unnamed x24, local copies, waits for them, and re-layouts  4.11 us
  transfers between devices with their start and end apart: 4, of which 4 were waited for; matrix products, arithmetic and copies ran while one was open for 5% of the time, Pallas kernels for 0%

commit v1 on v0

v1 whole, which is shorter than its diff:
```python
import functools

import jax
import jax.numpy as jnp
from jax import lax
from jax.experimental import pallas as pl
from jax.experimental.pallas import tpu as pltpu
from jax.sharding import PartitionSpec as P

MESH = pl.DeviceIdType.MESH
BF = jnp.bfloat16
F32 = jnp.float32
CAP = 5
LANES = 128
GROUPS = 4
MSG = 2 * CAP


def iota(shape, dim):
    return lax.broadcasted_iota(jnp.int32, shape, dim)


def dot(a, b):
    return jnp.dot(a, b, preferred_element_type=F32)


def dot_nt(a, b):
    return lax.dot_general(a, b, (((1,), (1,)), ((), ())), preferred_element_type=F32)


def dot_tn(a, b):
    return lax.dot_general(a, b, (((0,), (0,)), ((), ())), preferred_element_type=F32)


def div5(v):
    return (v * 205) >> 10


def kernel(
    nep, nx, ny, stage,
    tok_hbm, cot_hbm, routes_ref, mix_ref, gate_hbm, up_hbm, down_hbm,
    tg_ref, mg_ref, gt_ref, ut_ref, dg_ref,
    share, msg, rcv, rows, gate, up, down, acc, p8, aux, perm, bgu, hid,
    pown, psend, psib, sbr, sbl, rl, rr, mixv, mixs, ret, out,
    sh_sem, w_sem, d_send, d_recv, ag_rs, ag_rh, ag_ls, ag_lh, ag_ss, ag_l, ag_r, ag_s,
    ps_send, ps_recv, rs_send, rs_l, rs_r, mx_ss, mx_sr, mx_send, mx_recv, rt_send, rt_recv,
):
    e = lax.axis_index("ep")
    t = lax.axis_index("tp")
    x = t // 2
    c = t % 2
    nz = nep // ny
    z, y = e // ny, e % ny
    per = nep // GROUPS
    rpg = per * CAP
    tokn = share.shape[1]
    far = nx // 2

    def chip(d):
        return lax.rem(x + d + nx, nx)

    right = chip(1) * 2 + c
    left = chip(-1) * 2 + c
    sib = x * 2 + (1 - c)

    col = pl.multiple_of(t * LANES, LANES)
    share_copies = [
        pltpu.make_async_copy(tok_hbm.at[:, pl.ds(col, LANES)], share.at[0], sh_sem.at[0]),
        pltpu.make_async_copy(cot_hbm.at[:, pl.ds(col, LANES)], share.at[1], sh_sem.at[1]),
    ]
    for cp in share_copies:
        cp.start()
    weight_copies = [
        pltpu.make_async_copy(gate_hbm.at[0], gate, w_sem.at[0]),
        pltpu.make_async_copy(up_hbm.at[0], up, w_sem.at[1]),
        pltpu.make_async_copy(down_hbm.at[0], down, w_sem.at[2]),
    ]

    rcv[...] = jnp.zeros_like(rcv)
    mixv[...] = jnp.zeros_like(mixv)

    barrier = pltpu.get_barrier_semaphore()

    def order(j, n):
        half = (j + 1) // 2
        return lax.rem(n // 2 + (1 - 2 * (j % 2)) * half + n, n)

    def peer(j):
        dz, dy = order(j // ny, nz), order(j % ny, ny)
        return lax.rem(z + dz, nz) * ny + lax.rem(y + dy, ny)

    def greet(j, carry):
        pl.semaphore_signal(barrier, inc=1, device_id=(peer(j), t), device_id_type=MESH)
        return carry

    lax.fori_loop(0, nep - 1, greet, 0)
    for d in range(1, nx):
        pl.semaphore_signal(barrier, inc=1, device_id=(e, chip(d) * 2 + c), device_id_type=MESH)
    pl.semaphore_signal(barrier, inc=1, device_id=(e, sib), device_id_type=MESH)

    for cp in weight_copies:
        cp.start()

    r0, r1 = routes_ref[0:1, :], routes_ref[1:2, :]
    w = mix_ref[...].astype(F32)
    w0, w1 = w[0:1, :], w[1:2, :]
    upper = (iota((tokn, tokn), 0) < iota((tokn, tokn), 1)).astype(BF)
    er = iota((nep, tokn), 0)
    oh0, oh1 = er == r0, er == r1
    ranks = dot((oh0 | oh1).astype(BF), upper)
    aux[0:1, :] = jnp.sum(jnp.where(oh0, ranks, 0.0), axis=0, keepdims=True)
    aux[1:2, :] = jnp.sum(jnp.where(oh1, ranks, 0.0), axis=0, keepdims=True)

    blk = 128
    for b in range(nep * 8 // blk):
        rw = iota((blk, tokn), 0) + b * blk
        hit = ((rw >> 3) == r0) | ((rw >> 3) == r1)
        rk = dot(hit.astype(BF), upper)
        s = rw & 7
        p8[pl.ds(b * blk, blk), :] = (hit & (rk == s.astype(F32)) & (s < CAP)).astype(BF)

    pr, pc = iota((2 * rpg, 16 * per), 0), iota((2 * rpg, 16 * per), 1)
    second = pr >= rpg
    rr_ = pr - jnp.where(second, rpg, 0)
    src = div5(rr_)
    perm[...] = (pc == src * 16 + (rr_ - src * CAP) + jnp.where(second, CAP, 0)).astype(BF)

    for cp in share_copies:
        cp.wait()
    both = share[...].reshape(2 * tokn, LANES)
    blk = 256
    for b in range(nep * 16 // blk):
        rw = iota((blk, tokn), 0) + b * blk
        ex = rw >> 4
        q = rw & 15
        h0, h1 = ex == r0, ex == r1
        rk = dot((h0 | h1).astype(BF), upper)
        wt = jnp.where(h0, w0, 0.0) + jnp.where(h1, w1, 0.0)
        hit = h0 | h1
        one = jnp.where(hit & (rk == q.astype(F32)) & (q < CAP), 1.0, 0.0)
        two = jnp.where(hit & (rk == (q - CAP).astype(F32)) & (q >= CAP), wt, 0.0)
        sel = jnp.concatenate([one.astype(BF), two.astype(BF)], axis=1)
        msg[pl.ds(b * (blk // 16), blk // 16)] = dot(sel, both).astype(BF).reshape(blk // 16, 16, LANES)

    pl.semaphore_wait(barrier, nep - 1 + nx - 1 + 1)

    def give(j, carry):
        p = peer(j)
        pltpu.make_async_remote_copy(
            src_ref=msg.at[p, pl.ds(0, MSG)], dst_ref=rcv.at[e, pl.ds(0, MSG)],
            send_sem=d_send, recv_sem=d_recv.at[e // per],
            device_id=(p, t), device_id_type=MESH,
        ).start()
        return carry

    lax.fori_loop(0, nep - 1, give, 0)
    rcv[e] = msg[e]

    def remote(src, dst, ssem, rsem, to):
        return pltpu.make_async_remote_copy(
            src_ref=src, dst_ref=dst, send_sem=ssem, recv_sem=rsem, device_id=(e, to), device_id_type=MESH)

    def await_bytes(ref, sem):
        pltpu.make_async_copy(ref, ref, sem).wait()

    g0 = (e // per)

    def group(k):
        return lax.rem(g0 + k, GROUPS)

    def own(k):
        g = group(k)

        @pl.when(k == 0)
        def _():
            await_bytes(rcv.at[pl.ds(0, per - 1), pl.ds(0, MSG)], d_recv.at[g])

        @pl.when(k != 0)
        def _():
            await_bytes(rcv.at[pl.ds(0, per), pl.ds(0, MSG)], d_recv.at[g])

        got = rcv[pl.ds(g * per, per)].reshape(per * 16, LANES)
        rows[t, g] = dot(perm[...], got).astype(BF).reshape(2, rpg, LANES)
        unit = rows.at[t, g]
        remote(unit, unit, ag_rs, ag_l.at[0, g], right).start()
        remote(unit, unit, ag_ls, ag_r.at[0, g], left).start()
        remote(unit, unit, ag_ss, ag_s.at[0], sib).start()

    def passed(h, k):
        g = group(k)
        a, b = chip(-h) * 2 + c, chip(h) * 2 + c
        if h < far:
            ua, ub = rows.at[a, g], rows.at[b, g]
        else:
            ua, ub = rows.at[a, g, 0], rows.at[b, g, 1]
        await_bytes(ua, ag_l.at[h - 1, g])
        if h < far - 1:
            remote(ua, ua, ag_rs, ag_l.at[h, g], right).start()
        elif h == far - 1:
            remote(rows.at[a, g, 0], rows.at[a, g, 0], ag_rh, ag_l.at[h, g], right).start()
        await_bytes(ub, ag_r.at[h - 1, g])
        if h < far - 1:
            remote(ub, ub, ag_ls, ag_r.at[h, g], left).start()
        elif h == far - 1:
            remote(rows.at[b, g, 1], rows.at[b, g, 1], ag_lh, ag_r.at[h, g], left).start()
        remote(ua, ua, ag_ss, ag_s.at[nx - h], sib).start()
        remote(ub, ub, ag_ss, ag_s.at[h], sib).start()

    def sib_slice(d):
        s = chip(d) * 2 + (1 - c)
        await_bytes(rows.at[s], ag_s.at[d])

    def kstep(d, first=False):
        xc = chip(d)
        at = pl.multiple_of(xc * 2 * LANES, 2 * LANES)
        n = GROUPS * rpg

        def slab(which):
            return jnp.concatenate(
                [rows[2 * xc, :, which].reshape(n, LANES), rows[2 * xc + 1, :, which].reshape(n, LANES)], axis=1)

        wgu = jnp.concatenate([gate[pl.ds(at, 2 * LANES), :], up[pl.ds(at, 2 * LANES), :]], axis=1)
        a = dot(slab(0), wgu)
        b = dot_nt(slab(1), down[:, pl.ds(at, 2 * LANES)])
        if first:
            acc[:, 0:2 * LANES] = a
            acc[:, 2 * LANES:] = b
        else:
            acc[:, 0:2 * LANES] += a
            acc[:, 2 * LANES:] += b

    if stage >= 2:
        for s in range(GROUPS + far):
            if s < GROUPS:
                own(s)
            for h in range(1, far + 1):
                if 0 <= s - h < GROUPS:
                    passed(h, s - h)
            if s == GROUPS:
                for cp in weight_copies:
                    cp.wait()
                sib_slice(0)
                kstep(0, True)
            elif s > GROUPS:
                h = s - GROUPS
                sib_slice(h)
                kstep(h)
                sib_slice(nx - h)
                kstep(nx - h)
        sib_slice(far)
        kstep(far)
    else:
        for k in range(GROUPS):
            g = group(k)
            await_bytes(rcv.at[pl.ds(0, per - 1 if k == 0 else per), pl.ds(0, MSG)], d_recv.at[g])
        for cp in weight_copies:
            cp.wait()

    if stage >= 3:
        ones8 = [(iota((8, LANES), 0) == g).astype(BF) for g in range(GROUPS)]
        mixrow = jnp.zeros((8, rpg), F32)
        for g in range(GROUPS):
            rs = pl.ds(g * rpg, rpg)
            pg, pu, bh = acc[rs, 0:LANES], acc[rs, LANES:2 * LANES], acc[rs, 2 * LANES:]
            sig = jax.nn.sigmoid(pg)
            act = pg * sig
            hidden = (act * pu).astype(BF)
            hid[rs, :] = hidden
            hb = hidden.astype(F32) * bh
            hi = hb.astype(BF)
            lo = (hb - hi.astype(F32)).astype(BF)
            mixrow = mixrow + dot_nt(ones8[g], hi) + dot_nt(ones8[g], lo)
            bgu[rs, 0:LANES] = (bh * pu * (sig * (1.0 + pg * (1.0 - sig)))).astype(BF)
            bgu[rs, LANES:] = (bh * act).astype(BF)
        mixs[0, :, 0:rpg] = mixrow[0:GROUPS, :]
        mixs[0, :, rpg:] = jnp.zeros((GROUPS, LANES - rpg), F32)
        remote(mixs.at[0], mixs.at[1], mx_ss, mx_sr, sib).start()

    def part(d):
        xc = chip(d)
        at = pl.multiple_of(xc * 2 * LANES, 2 * LANES)
        wgu = jnp.concatenate([gate[pl.ds(at, 2 * LANES), :], up[pl.ds(at, 2 * LANES), :]], axis=1)
        v = dot_nt(bgu[...], wgu)
        a, b = v[:, 0:LANES], v[:, LANES:]
        pown[d % nx] = jnp.where(c == 0, a, b)
        psend[d % nx] = jnp.where(c == 0, b, a).astype(BF)
        remote(psend.at[d % nx], psib.at[d % nx], ps_send, ps_recv.at[d % nx], sib).start()

    def get_sib(d):
        await_bytes(psib.at[d % nx], ps_recv.at[d % nx])

    def both_cores(d, u):
        rs = pl.ds(u * rpg, rpg)
        return pown[d % nx, rs, :] + psib[d % nx, rs, :].astype(F32)

    def send_rs(val, buf, sem_of, step, u, to):
        buf[step - 1, u] = val.astype(BF)
        here = 0 if buf is sbr else 1
        return remote(buf.at[step - 1, u], (rr if here else rl).at[step - 1, u], rs_send.at[here, step - 1], sem_of.at[step - 1, u], to)

    def grads(xs):
        xc = xs
        n = GROUPS * rpg
        at = xs * 2 * LANES

        def slab(which):
            return jnp.concatenate(
                [rows[2 * xc, :, which].reshape(n, LANES), rows[2 * xc + 1, :, which].reshape(n, LANES)], axis=1)

        v = dot_tn(bgu[...], slab(0))
        gt_ref[:, at:at + 2 * LANES] = v[0:LANES].astype(BF)
        ut_ref[:, at:at + 2 * LANES] = v[LANES:].astype(BF)
        dg_ref[:, at:at + 2 * LANES] = dot_tn(hid[...], slab(1)).astype(BF)

    if stage >= 4:
        half = GROUPS // 2
        part(far)
        part(far - 1)
        part(1 - far)
        await_bytes(mixs.at[1], mx_sr)
        mixv[0] = mixs[0] + mixs[1]

        def tell(d, carry):
            remote(mixv.at[0], mixv.at[d], mx_send, mx_recv, chip(d) * 2 + c).start()
            return carry

        for d in range(1, nx):
            remote(mixv.at[0], mixv.at[d], mx_send, mx_recv, chip(d) * 2 + c).start()
        get_sib(far)
        for u in range(half):
            send_rs(both_cores(far, u), sbr, rs_l, 1, u, right).start()
            send_rs(both_cores(far, u + half), sbl, rs_r, 1, u + half, left).start()
        for step in range(2, far + 1):
            d = far + 1 - step
            if d > 1:
                part(d - 1)
                part(1 - d)
            elif d == 1:
                part(0)
            get_sib(d)
            get_sib(-d)
            ro = range(GROUPS) if step > 2 else [2, 3, 0, 1]
            lo_ = range(GROUPS)
            for ur, ul in zip(ro, lo_):
                v = both_cores(d, ur)
                if step > 2 or ur < half:
                    await_bytes(rl.at[step - 2, ur], rs_l.at[step - 2, ur])
                    v = v + rl[step - 2, ur].astype(F32)
                send_rs(v, sbr, rs_l, step, ur, right).start()
                v = both_cores(-d, ul)
                if step > 2 or ul >= half:
                    await_bytes(rr.at[step - 2, ul], rs_r.at[step - 2, ul])
                    v = v + rr[step - 2, ul].astype(F32)
                send_rs(v, sbl, rs_r, step, ul, left).start()
            grads(2 * step - 4)
            grads(2 * step - 3)
        get_sib(0)
        for i in range(2 * far - 2, nx):
            grads(i)
        await_bytes(mixv.at[pl.ds(0, nx - 1)], mx_recv)
        total_mix = mixv[0]
        for d in range(1, nx):
            total_mix = total_mix + mixv[d]
        mhi = total_mix.astype(BF).astype(F32)
        mlo = total_mix - mhi

        br, bc = iota((LANES, LANES), 0), iota((LANES, LANES), 1)
        src_of = div5(bc)
        slot_of = bc - src_of * CAP
        valid = bc < rpg
        spread = (((br >> 3) == src_of) & ((br & 7) == slot_of) & valid)[:, 0:rpg].astype(BF)
        take = ((br >> 3) == src_of) & ((br & 7) == CAP) & valid
        src_r = div5(br)
        slot_r = br - src_r * CAP
        bhi = (bc == slot_r).astype(BF)
        blo = (bc == slot_r + 8).astype(BF)

        for u in range(GROUPS):
            await_bytes(rl.at[far - 1, u], rs_l.at[far - 1, u])
            await_bytes(rr.at[far - 1, u], rs_r.at[far - 1, u])
            v = both_cores(0, u) + rl[far - 1, u].astype(F32) + rr[far - 1, u].astype(F32)
            m = dot(spread, v.astype(BF))
            m = m + dot(jnp.where(take, mhi[u:u + 1, :], 0.0).astype(BF), bhi)
            m = m + dot(jnp.where(take, mlo[u:u + 1, :], 0.0).astype(BF), blo)
            out[pl.ds(u * per, per)] = m.astype(BF).reshape(per, 8, LANES)

            def back(j, carry):
                i = u * per + j

                @pl.when(i != e)
                def _():
                    pltpu.make_async_remote_copy(
                        src_ref=out.at[i], dst_ref=ret.at[e], send_sem=rt_send, recv_sem=rt_recv,
                        device_id=(i, t), device_id_type=MESH,
                    ).start()
                return carry

            lax.fori_loop(0, per, back, 0)
        ret[e] = out[e]
        await_bytes(ret.at[pl.ds(0, nep - 1)], rt_recv)

        back_rows = ret[...].reshape(nep * 8, LANES)
        tg_ref[...] = dot_tn(p8[...], back_rows).astype(BF)
        sr, sc = iota((nep, nep * 8), 0), iota((nep, nep * 8), 1)
        mixes = dot((sc == sr * 8 + CAP).astype(BF), back_rows).astype(BF)
        lane = iota((LANES, tokn), 0).astype(F32)
        done = []
        for k, (oh, wk) in enumerate(((oh0, w0), (oh1, w1))):
            seen = dot_tn(mixes, oh.astype(BF))
            rank = aux[k:k + 1, :]
            picked = jnp.where((lane == rank) | (lane == rank + 8.0), seen, 0.0)
            done.append(jnp.sum(picked, axis=0, keepdims=True) / wk)
        mg_ref[...] = jnp.concatenate(done, axis=0).astype(BF)

    await_bytes(msg.at[pl.ds(0, nep - 1), pl.ds(0, MSG)], d_send)
    if stage >= 2:
        await_bytes(rows.at[pl.ds(0, far - 1)], ag_rs)
        await_bytes(rows.at[pl.ds(0, far - 1)], ag_ls)
        await_bytes(rows.at[0, :, 0], ag_rh)
        await_bytes(rows.at[0, :, 0], ag_lh)
        await_bytes(rows.at[pl.ds(0, nx)], ag_ss)
    if stage >= 3:
        await_bytes(mixs.at[0], mx_ss)
    if stage == 3:
        await_bytes(mixs.at[1], mx_sr)
    if stage >= 4:
        await_bytes(psend, ps_send)
        await_bytes(mixv.at[pl.ds(0, nx - 1)], mx_send)
        await_bytes(sbr.at[0, pl.ds(0, half)], rs_send.at[0, 0])
        await_bytes(sbl.at[0, pl.ds(half, half)], rs_send.at[1, 0])
        for step in range(1, far):
            await_bytes(sbr.at[step], rs_send.at[0, step])
            await_bytes(sbl.at[step], rs_send.at[1, step])
        await_bytes(out.at[pl.ds(0, nep - 1)], rt_send)


def solution(mesh):
    nep, ntp = mesh.shape["ep"], mesh.shape["tp"]
    nx = ntp // 2
    ny = 8 if nep == 64 else 4

    def on_device(tokens, cotangent, mix_weights, routes, gate_proj, up_proj, down_proj):
        tokn, width = tokens.shape
        ff = gate_proj.shape[2]
        n = nep * CAP
        per = nep // GROUPS
        rpg = per * CAP
        far = nx // 2
        vm = pl.BlockSpec(memory_space=pltpu.VMEM)
        hbm = pl.BlockSpec(memory_space=pl.ANY)
        dma = pltpu.SemaphoreType.DMA
        tg, mg, gt, ut, dg = pl.pallas_call(
            functools.partial(kernel, nep, nx, ny, 4),
            out_shape=(
                jax.ShapeDtypeStruct((tokn, LANES), BF),
                jax.ShapeDtypeStruct((2, tokn), BF),
                jax.ShapeDtypeStruct((ff, width), BF),
                jax.ShapeDtypeStruct((ff, width), BF),
                jax.ShapeDtypeStruct((ff, width), BF),
            ),
            in_specs=[hbm, hbm, vm, vm, hbm, hbm, hbm],
            out_specs=[vm] * 5,
            scratch_shapes=[
                pltpu.VMEM((2, tokn, LANES), BF),
                pltpu.VMEM((nep, 16, LANES), BF),
                pltpu.VMEM((nep, 16, LANES), BF),
                pltpu.VMEM((ntp, GROUPS, 2, rpg, LANES), BF),
                pltpu.VMEM((width, ff), BF),
                pltpu.VMEM((width, ff), BF),
                pltpu.VMEM((ff, width), BF),
                pltpu.VMEM((n, 3 * LANES), F32),
                pltpu.VMEM((nep * 8, tokn), BF),
                pltpu.VMEM((8, tokn), F32),
                pltpu.VMEM((2 * rpg, 16 * per), BF),
                pltpu.VMEM((n, 2 * LANES), BF),
                pltpu.VMEM((n, LANES), BF),
                pltpu.VMEM((nx, n, LANES), F32),
                pltpu.VMEM((nx, n, LANES), BF),
                pltpu.VMEM((nx, n, LANES), BF),
                pltpu.VMEM((far, GROUPS, rpg, LANES), BF),
                pltpu.VMEM((far, GROUPS, rpg, LANES), BF),
                pltpu.VMEM((far, GROUPS, rpg, LANES), BF),
                pltpu.VMEM((far, GROUPS, rpg, LANES), BF),
                pltpu.VMEM((nx, GROUPS, LANES), F32),
                pltpu.VMEM((2, GROUPS, LANES), F32),
                pltpu.VMEM((nep, 8, LANES), BF),
                pltpu.VMEM((nep, 8, LANES), BF),
                dma((2,)), dma((3,)), dma, dma((GROUPS,)),
                dma, dma, dma, dma, dma,
                dma((far, GROUPS)), dma((far, GROUPS)), dma((nx,)),
                dma, dma((nx,)), dma((2, far)), dma((far, GROUPS)), dma((far, GROUPS)),
                dma, dma, dma, dma, dma, dma,
            ],
            compiler_params=pltpu.CompilerParams(
                collective_id=0, has_side_effects=True, vmem_limit_bytes=48 * 1024 * 1024),
        )(tokens, cotangent, routes.T, mix_weights.T, gate_proj, up_proj, down_proj)
        return tg, mg.T, gt.T[None], ut.T[None], dg[None]

    in_specs = (
        P("ep", None), P("ep", None), P("ep", None), P("ep", None),
        P("ep", None, "tp"), P("ep", None, "tp"), P("ep", "tp", None),
    )
    out_specs = (
        P("ep", "tp"), P("ep", None), P("ep", None, "tp"), P("ep", None, "tp"), P("ep", "tp", None),
    )
    return jax.shard_map(on_device, mesh=mesh, in_specs=in_specs, out_specs=out_specs, check_vma=False)
```

time: 204 us -> 87.3 us (0.43)
  the two profiles are of different devices: /device:TPU:1 before, /device:TPU:4 now
where the time goes in v1:
time: 87.3 us; the launch traced here: 86.9 us
  Pallas kernels  76.4 us (88%)
  local copies, waits for them, and re-layouts  9.79 us (11%)
    pallas_call x1, Pallas kernels, on_device(): pl.pallas_call(functools.partial(kernel, nep, nx, ny, 4), out_shape=(jax....  76.4 us
    unnamed x19, local copies, waits for them, and re-layouts  9.79 us

profile of v1, /device:TPU:4, one launch (start us, length us, event | category | flops | bytes accessed | tf_op | source)
XLA Modules:
  0.0 86.9 jit_solution(11073566839592546135)
XLA Ops:
  0.6 0.0 copy-start.5
  0.6 0.0 copy-start.6
  0.7 0.7 copy-done.5
  1.3 0.0 copy-done.6
  1.3 0.0 copy-start
  1.3 1.0 %copy-done = bf16[128,2048]{1,0:T(8,128)(2,1)S(1)} copy-done((bf16[128,2048]{1,0:T(8,128)(2,1)S(1)}, bf16[128,2048]{1,0:T(8,128)(2,1)}, u32[]{:S(2)}) %copy-start) | copy-done | bytes 524312
  2.4 0.0 copy-start.1
  2.4 1.0 %copy-done.1 = bf16[128,2048]{1,0:T(8,128)(2,1)S(1)} copy-done((bf16[128,2048]{1,0:T(8,128)(2,1)S(1)}, bf16[128,2048]{1,0:T(8,128)(2,1)}, u32[]{:S(2)}) %copy-start.1) | copy-done | bytes 524312
  3.4 0.0 copy-start.2
  3.4 1.0 %copy-done.2 = bf16[1,2048,128]{2,1,0:T(8,128)(2,1)S(1)} copy-done((bf16[1,2048,128]{2,1,0:T(8,128)(2,1)S(1)}, bf16[1,2048,128]{2,1,0:T(8,128)(2,1)}, u32[]{:S(2)}) %copy-start.2) | copy-done | bytes 524312
  4.4 0.0 copy-start.3
  4.4 1.0 %copy-done.3 = bf16[1,2048,128]{2,1,0:T(8,128)(2,1)S(1)} copy-done((bf16[1,2048,128]{2,1,0:T(8,128)(2,1)S(1)}, bf16[1,2048,128]{2,1,0:T(8,128)(2,1)}, u32[]{:S(2)}) %copy-start.3) | copy-done | bytes 524312
  5.5 0.0 copy-start.4
  5.5 1.0 %copy-done.4 = bf16[1,128,2048]{2,1,0:T(8,128)(2,1)S(1)} copy-done((bf16[1,128,2048]{2,1,0:T(8,128)(2,1)S(1)}, bf16[1,128,2048]{2,1,0:T(8,128)(2,1)}, u32[]{:S(2)}) %copy-start.4) | copy-done | bytes 524312
  6.5 76.4 %shard_map.110 = (bf16[128,128]{1,0:T(8,128)(2,1)S(1)}, bf16[2,128]{1,0:T(2,128)(2,1)S(1)}, bf16[128,2048]{1,0:T(8,128)(2,1)S(1)}, bf16[128,2048]{1,0:T(8,128)(2,1)S(1)}, bf16[128,2048]{1,0:T(8,128)(2,1)S(1)}) custom-call(bf16[128,2048]{1,0:T(8,128)(2,1)S(1)} %copy-done, bf16[128,2048]{1,0:T(8,128)(2,1)S(1)} %copy-done.1, s32[2,128]{1,0:T(2,128)S(1)} %bitcast.13, ...), custom_call_target="tpu_custom_call" | custom-call | tf_op jit(solution)/shard_map/pallas_call | solution.py:452
  82.9 1.0 %copy.12 = bf16[1,2048,128]{2,1,0:T(8,128)(2,1)} copy(bf16[1,2048,128]{1,2,0:T(8,128)(2,1)S(1)} %bitcast.12) | data formatting | bytes 1048576
  83.9 1.0 %copy.13 = bf16[1,2048,128]{2,1,0:T(8,128)(2,1)} copy(bf16[1,2048,128]{1,2,0:T(8,128)(2,1)S(1)} %bitcast.11) | data formatting | bytes 1048576
  84.9 0.6 copy.17
  85.6 0.5 copy.18
  86.1 0.8 copy.19
Async XLA Ops:
  0.6 0.7 copy-start.5
  0.6 0.7 copy-start.6
  1.3 1.0 %copy-start = (bf16[128,2048]{1,0:T(8,128)(2,1)S(1)}, bf16[128,2048]{1,0:T(8,128)(2,1)}, u32[]{:S(2)}) copy-start(bf16[128,2048]{1,0:T(8,128)(2,1)} %tok_hbm.1) | copy-start | bytes 1572868
  2.4 1.0 %copy-start.1 = (bf16[128,2048]{1,0:T(8,128)(2,1)S(1)}, bf16[128,2048]{1,0:T(8,128)(2,1)}, u32[]{:S(2)}) copy-start(bf16[128,2048]{1,0:T(8,128)(2,1)} %cot_hbm.1) | copy-start | bytes 1572868
  3.4 1.0 %copy-start.2 = (bf16[1,2048,128]{2,1,0:T(8,128)(2,1)S(1)}, bf16[1,2048,128]{2,1,0:T(8,128)(2,1)}, u32[]{:S(2)}) copy-start(bf16[1,2048,128]{2,1,0:T(8,128)(2,1)} %gate_hbm.1) | copy-start | bytes 1572868
  4.4 1.0 %copy-start.3 = (bf16[1,2048,128]{2,1,0:T(8,128)(2,1)S(1)}, bf16[1,2048,128]{2,1,0:T(8,128)(2,1)}, u32[]{:S(2)}) copy-start(bf16[1,2048,128]{2,1,0:T(8,128)(2,1)} %up_hbm.1) | copy-start | bytes 1572868
  5.5 1.0 %copy-start.4 = (bf16[1,128,2048]{2,1,0:T(8,128)(2,1)S(1)}, bf16[1,128,2048]{2,1,0:T(8,128)(2,1)}, u32[]{:S(2)}) copy-start(bf16[1,128,2048]{2,1,0:T(8,128)(2,1)} %down_hbm.1) | copy-start | bytes 1572868

commit v2 on v0

v2 whole, which is shorter than its diff:
```python
import functools

import jax
import jax.numpy as jnp
from jax import lax
from jax.experimental import pallas as pl
from jax.experimental.pallas import tpu as pltpu
from jax.sharding import PartitionSpec as P

MESH = pl.DeviceIdType.MESH
BF = jnp.bfloat16
F32 = jnp.float32
CAP = 5
MSG = 2 * CAP
LANES = 128
NX = NY = NZ = 8
GROUPS = 4
ZB = NZ // GROUPS
HY = NY // 2
PER = ZB * HY
RPG = PER * CAP
TILE = 2 * RPG + 8
CUT = 40
WIDE = 2 * LANES
QUADS = 4
QUAD = 4 * LANES
DIRECT = ()
EARLY = "W r0 r1 r2 s3 A0 A1 B0 t3 B1 P0 A2 H0 C0 A3 P1 B2 H1 P2 E0 B3 P3 H2 C2 F0 C1 H3 C3 E2 E1 E3 F2 F1 F3 T G"
LATE = "W r0 A0 r1 r2 r3 B0 P0 A3 A1 H0 C0 A2 B1 P1 E0 H1 C1 B2 B3 F0 P2 E1 H2 C2 P3 H3 C3 F1 E2 E3 F2 F3 T G"


def iota(shape, dim):
    return lax.broadcasted_iota(jnp.int32, shape, dim)


def dot(a, b):
    return jnp.dot(a, b, preferred_element_type=F32)


def dot_nt(a, b):
    return lax.dot_general(a, b, (((1,), (1,)), ((), ())), preferred_element_type=F32)


def dot_tn(a, b):
    return lax.dot_general(a, b, (((0,), (0,)), ((), ())), preferred_element_type=F32)


def div5(v):
    return (v * 205) >> 10


def kernel(
    tok_hbm, cot_hbm, routes_hbm, mix_hbm, gate_hbm, up_hbm, down_hbm,
    ret, p8, aux, gg_ref, ug_ref, dg_ref,
    routes_ref, mix_ref, share, msg, ybuf, zbuf, rows, w4, dw, w4t, dwt, perm, bgu, hid, obgu, ohid, mixt,
    pre, back, pown, sb, rb, out,
    ready, t_sem, sh_sem, w_sem, x_sem, y_send, y_recv, z_send, z_recv, ag_send, ag_recv, sib_send, sib_recv,
    bh_send, bh_recv, rs_send, rs_recv, rt_send, rt_recv,
):
    e = lax.axis_index("ep")
    t = lax.axis_index("tp")
    z, y = e // NY, e % NY
    x, c = t // 2, t % 2
    tokn = share.shape[1]
    nep = NZ * NY
    active = y % 2 == c

    def chip(d):
        return lax.rem(x + d + NX, NX)

    def quad(d):
        return lax.rem(x + d + NX, QUADS)

    sib = (e, x * 2 + (1 - c))

    def along_x(d):
        return (e, chip(d) * 2 + c)

    def remote(src, dst, ssem, rsem, to):
        return pltpu.make_async_remote_copy(
            src_ref=src, dst_ref=dst, send_sem=ssem, recv_sem=rsem, device_id=to, device_id_type=MESH)

    def await_bytes(ref, sem):
        pltpu.make_async_copy(ref, ref, sem).wait()

    col = pl.multiple_of(quad(0) * QUAD, QUAD)
    table_copies = [
        pltpu.make_async_copy(routes_hbm, routes_ref, t_sem.at[0]),
        pltpu.make_async_copy(mix_hbm, mix_ref, t_sem.at[1]),
    ]
    share_copies = [
        pltpu.make_async_copy(tok_hbm.at[:, pl.ds(col, QUAD)], share.at[0], sh_sem.at[0]),
        pltpu.make_async_copy(cot_hbm.at[:, pl.ds(col, QUAD)], share.at[1], sh_sem.at[1]),
    ]
    lane = pl.multiple_of(c * WIDE, WIDE)
    ours = w4.at[:, pl.ds(lane, WIDE)]
    downs = dw.at[pl.ds(pl.multiple_of(c * LANES, LANES), LANES)]
    weight_copies = [
        pltpu.make_async_copy(gate_hbm.at[0], w4.at[:, pl.ds(lane, LANES)], w_sem.at[0]),
        pltpu.make_async_copy(up_hbm.at[0], w4.at[:, pl.ds(pl.multiple_of(lane + LANES, LANES), LANES)], w_sem.at[1]),
        pltpu.make_async_copy(down_hbm.at[0], downs, w_sem.at[2]),
    ]
    weight_moves = [
        remote(ours, ours, x_sem.at[0], x_sem.at[1], sib),
        remote(downs, downs, x_sem.at[2], x_sem.at[3], sib),
    ]
    barrier = pltpu.get_barrier_semaphore()
    for d in (4, 3, 5, 2, 6, 1, 7):
        pl.semaphore_signal(barrier, inc=1, device_id=(z * NY + lax.rem(y + d, NY), t), device_id_type=MESH)
    for d in (2, -2, 1, -1):
        pl.semaphore_signal(barrier, inc=1, device_id=along_x(d), device_id_type=MESH)
    pl.semaphore_signal(barrier, inc=1, device_id=sib, device_id_type=MESH)
    for cp in table_copies + share_copies + weight_copies:
        cp.start()
    with jax.named_scope("barrier"):
        pl.semaphore_wait(barrier, 12 + jnp.where(z > 0, 1, 0))

    @pl.when(z < NZ - 1)
    def _():
        pl.semaphore_signal(barrier, inc=1, device_id=(e + NY, t), device_id_type=MESH)

    for zz in range(NZ - 1):
        @pl.when(zz < z)
        def _():
            pl.semaphore_signal(ready.at[z], inc=1, device_id=(zz * NY + y, t), device_id_type=MESH)

    for cp in table_copies:
        cp.wait()
    r0, r1 = routes_ref[0:1, :], routes_ref[1:2, :]
    w = mix_ref[...].astype(F32)
    w0, w1 = w[0:1, :], w[1:2, :]
    upper = (iota((tokn, tokn), 0) < iota((tokn, tokn), 1)).astype(BF)
    with jax.named_scope("share"):
        for cp in share_copies:
            cp.wait()

    @pl.when(active)
    def _():
        both = share[...].reshape(2 * tokn, QUAD)
        blk = ZB * NY * 16
        for b in range(GROUPS):
            rw = iota((blk, tokn), 0) + b * blk
            ex = rw >> 4
            q = rw & 15
            h0, h1 = ex == r0, ex == r1
            hit = h0 | h1
            rk = dot(hit.astype(BF), upper)
            wt = jnp.where(h0, w0, 0.0) + jnp.where(h1, w1, 0.0)
            one = jnp.where(hit & (rk == q.astype(F32)) & (q < CAP), 1.0, 0.0)
            two = jnp.where(hit & (rk == (q - CAP).astype(F32)) & (q >= CAP), wt, 0.0)
            sel = jnp.concatenate([one.astype(BF), two.astype(BF)], axis=1)
            v = dot(sel, both).astype(BF)
            for ch in range(4):
                msg[pl.ds(b * ZB, ZB), :, ch] = v[:, ch * LANES:(ch + 1) * LANES].reshape(ZB, NY, 16, LANES)
            for d in (4, 3, 5, 2, 6, 1, 7):
                yd = lax.rem(y + d, NY)
                remote(
                    msg.at[pl.ds(b * ZB, ZB), yd, :, pl.ds(0, MSG)],
                    ybuf.at[pl.ds(b * ZB, ZB), y // 2, :, pl.ds(0, MSG)],
                    y_send, y_recv.at[b], (z * NY + yd, t)).start()
            ybuf[pl.ds(b * ZB, ZB), y // 2] = msg[pl.ds(b * ZB, ZB), y]

    for cp in weight_copies:
        cp.wait()
    for cp in weight_moves:
        cp.start()

    def relay(b):
        with jax.named_scope(f"ywait{b}"):
            @pl.when(active)
            def _():
                await_bytes(ybuf.at[pl.ds(b * ZB, ZB), pl.ds(0, HY - 1), :, pl.ds(0, MSG)], y_recv.at[b])

            @pl.when(jnp.logical_not(active))
            def _():
                await_bytes(ybuf.at[pl.ds(b * ZB, ZB), :, :, pl.ds(0, MSG)], y_recv.at[b])
        for zd in range(b * ZB, (b + 1) * ZB):
            @pl.when(zd == z)
            def _():
                zbuf[zd] = ybuf[zd]

            @pl.when(zd > z)
            def _():
                with jax.named_scope(f"ready{zd}"):
                    pl.semaphore_wait(ready.at[zd], 1)

            @pl.when(zd != z)
            def _():
                remote(
                    ybuf.at[zd, :, :, pl.ds(0, MSG)], zbuf.at[z, :, :, pl.ds(0, MSG)],
                    z_send, z_recv.at[z], (zd * NY + y, t)).start()

    def unit(d, g):
        return rows.at[c, quad(d), :, pl.ds(g * RPG, RPG)]

    def half(d, g, i):
        return rows.at[c, quad(d), i, pl.ds(g * RPG, RPG)]

    def to_sib(d, g):
        u = unit(d, g)
        remote(u, u, sib_send, sib_recv, sib).start()

    def gather_out(g):
        for zs in range(g * ZB, (g + 1) * ZB):
            @pl.when(zs != z)
            def _():
                with jax.named_scope(f"zwait{zs}"):
                    await_bytes(zbuf.at[zs, :, :, pl.ds(0, MSG)], z_recv.at[zs])
        got = jnp.concatenate(
            [zbuf[pl.ds(g * ZB, ZB), :, ch].reshape(PER * 16, LANES) for ch in range(4)], axis=1)
        got = jnp.where((iota(got.shape, 0) & 15) < MSG, got, jnp.zeros_like(got))
        v = dot(perm[...], got)
        rows[c, quad(0), 0, g * RPG:(g + 1) * RPG] = v[0:RPG].astype(BF)
        rows[c, quad(0), 1, g * RPG:(g + 1) * RPG] = v[RPG:].astype(BF)
        u = unit(0, g)
        remote(u, u, ag_send, ag_recv.at[0, g], along_x(1)).start()
        remote(u, u, ag_send, ag_recv.at[1, g], along_x(-1)).start()
        if g in DIRECT:
            for i, d in ((0, 2), (1, -2)):
                h = half(0, g, i)
                remote(h, h, ag_send, ag_recv.at[2 + i, g], along_x(d)).start()
        to_sib(0, g)

    def gather_in(g):
        for i, d in ((0, -1), (1, 1)):
            await_bytes(unit(d, g), ag_recv.at[i, g])
            if g not in DIRECT:
                h = half(d, g, i)
                remote(h, h, ag_send, ag_recv.at[2 + i, g], along_x(-d)).start()
            to_sib(d, g)

    def gather_far(g):
        for i in range(2):
            await_bytes(half(2, g, i), ag_recv.at[2 + i, g])
        to_sib(2, g)

    def send_part(g, i, to):
        remote(sb.at[g, i], rb.at[g, i], rs_send, rs_recv.at[g, i], along_x(to)).start()

    near, past = pl.ds(0, CUT), pl.ds(CUT, TILE - CUT)

    def products(g, d):
        at = pl.ds(g * RPG, RPG)
        q = quad(d)
        features = pl.ds(pl.multiple_of(q * QUAD, QUAD), QUAD)
        return dot(rows[c, q, 0, at], w4[features, :]), dot(rows[c, q, 1, at], dwt[features, :])

    def first_products(g):
        each = [products(g, d) for d in (0, -1, 1)]
        pre[g] = each[0][0] + each[1][0] + each[2][0]
        back[g] = each[0][1] + each[1][1] + each[2][1]

    def compute(g):
        at = pl.ds(g * RPG, RPG)
        pgu, bh = products(g, 2)
        pgu = pgu + pre[g]
        bh = bh + back[g]
        pg = jnp.concatenate([pgu[:, 0:LANES], pgu[:, WIDE:WIDE + LANES]], axis=1)
        pu = jnp.concatenate([pgu[:, LANES:WIDE], pgu[:, WIDE + LANES:]], axis=1)
        sig = jax.nn.sigmoid(pg)
        act = pg * sig
        hidden = (act * pu).astype(BF)
        bg = (bh * pu * (sig * (1.0 + pg * (1.0 - sig)))).astype(BF)
        bu = (bh * act).astype(BF)
        b0 = jnp.concatenate([bg[:, 0:LANES], bu[:, 0:LANES]], axis=1)
        b1 = jnp.concatenate([bg[:, LANES:], bu[:, LANES:]], axis=1)
        b4 = jnp.concatenate([b0, b1], axis=1)
        hb = hidden.astype(F32) * bh
        hi = hb.astype(BF)
        lo = (hb - hi.astype(F32)).astype(BF)
        ones = jnp.ones((8, WIDE), BF)
        sums = dot_nt(ones, hi) + dot_nt(ones, lo)
        shi = sums.astype(BF).astype(F32)
        row = iota((8, RPG), 0)
        mixt[g, :, 0:RPG] = jnp.where(row == 0, shi, jnp.where(row == 1, sums - shi, 0.0))
        tile = mixt[g].astype(BF)
        for d, i, to in ((3, 0, 1), (5, 1, -1), (4, 4, 0), (1, 2, 1), (7, 3, -1), (2, 0, None), (6, 1, None), (0, 2, None)):
            cols = pl.ds(pl.multiple_of(chip(d) * WIDE, WIDE), WIDE)
            v = dot(b4, w4t[:, cols])
            if to is None:
                pown[g, i, 0:RPG] = v[:, 0:LANES]
                pown[g, i, RPG:2 * RPG] = v[:, LANES:]
            else:
                sb[g, i, 0:RPG] = v[:, 0:LANES].astype(BF)
                sb[g, i, RPG:2 * RPG] = v[:, LANES:].astype(BF)
                sb[g, i, 2 * RPG:] = tile
                if to:
                    send_part(g, i, to)
                else:
                    remote(sb.at[g, 4, near], rb.at[g, 4, near], rs_send, rs_recv.at[g, 4], along_x(2)).start()
                    remote(sb.at[g, 4, past], rb.at[g, 4, past], rs_send, rs_recv.at[g, 7], along_x(-2)).start()
        first = c == 0
        bgu[c, at] = jnp.where(first, b0.astype(F32), b1.astype(F32)).astype(BF)
        obgu[g] = jnp.where(first, b1.astype(F32), b0.astype(F32)).astype(BF)
        hf = hidden.astype(F32)
        hid[c, at] = jnp.where(first, hf[:, 0:LANES], hf[:, LANES:]).astype(BF)
        ohid[g] = jnp.where(first, hf[:, LANES:], hf[:, 0:LANES]).astype(BF)
        remote(obgu.at[g], bgu.at[c, at], bh_send.at[0], bh_recv.at[0], sib).start()
        remote(ohid.at[g], hid.at[c, at], bh_send.at[1], bh_recv.at[1], sib).start()

    def chunk(g, i):
        return jnp.concatenate([pown[g, i], mixt[g]], axis=0)

    def scatter_two(g):
        await_bytes(rb.at[g, 0], rs_recv.at[g, 0])
        await_bytes(rb.at[g, 4, near], rs_recv.at[g, 4])
        v = chunk(g, 0) + rb[g, 0].astype(F32)
        sb[g, 5, 0:CUT] = (v[0:CUT] + rb[g, 4, 0:CUT].astype(F32)).astype(BF)
        sb[g, 5, CUT:] = v[CUT:].astype(BF)
        send_part(g, 5, 2)
        await_bytes(rb.at[g, 1], rs_recv.at[g, 1])
        await_bytes(rb.at[g, 4, past], rs_recv.at[g, 7])
        v = chunk(g, 1) + rb[g, 1].astype(F32)
        sb[g, 6, 0:CUT] = v[0:CUT].astype(BF)
        sb[g, 6, CUT:] = (v[CUT:] + rb[g, 4, CUT:].astype(F32)).astype(BF)
        send_part(g, 6, -2)

    def give_back(g):
        v = chunk(g, 2)
        for i in (2, 3, 5, 6):
            await_bytes(rb.at[g, i], rs_recv.at[g, i])
            v = v + rb[g, i].astype(F32)
        sums = v[2 * RPG:2 * RPG + 1] + v[2 * RPG + 1:2 * RPG + 2]
        mhi = sums.astype(BF).astype(F32)
        mlo = sums - mhi
        br, bc = iota((LANES, LANES), 0), iota((LANES, LANES), 1)
        second = bc >= RPG
        row = bc - jnp.where(second, RPG, 0)
        src_of = div5(row)
        slot_of = row - src_of * CAP
        here = ((br >> 3) == src_of + jnp.where(second, PER, 0)) & (bc < 2 * RPG)
        spread = (here & ((br & 7) == slot_of))[:, 0:2 * RPG].astype(BF)
        take = (((br >> 3) & (PER - 1)) == div5(bc)) & ((br & 7) == CAP) & (bc < RPG)
        slot_r = br - div5(br) * CAP
        m = dot(spread, v[0:2 * RPG].astype(BF))
        m = m + dot(jnp.where(take, mhi, 0.0).astype(BF), (bc == slot_r).astype(BF))
        m = m + dot(jnp.where(take, mlo, 0.0).astype(BF), (bc == slot_r + 8).astype(BF))
        out[g] = m.astype(BF).reshape(2, PER, 8, LANES)
        for j in range(PER):
            i = (g * ZB + j // HY) * NY + 2 * (j % HY) + c
            for hf in range(2):
                here_ = (i == e) & (c == hf)

                @pl.when(here_)
                def _():
                    ret[e] = out[g, hf, j]

                @pl.when(jnp.logical_not(here_))
                def _():
                    remote(out.at[g, hf, j], ret.at[e], rt_send, rt_recv, (i, x * 2 + hf)).start()

    def grads():
        await_bytes(rows.at[1 - c], sib_recv)
        await_bytes(bgu.at[1 - c], bh_recv.at[0])
        await_bytes(hid.at[1 - c], bh_recv.at[1])
        for q in range(QUADS):
            at = slice(q * QUAD, (q + 1) * QUAD)
            v = dot_tn(rows[0, q, 0], bgu[0]) + dot_tn(rows[1, q, 0], bgu[1])
            gg_ref[at, :] = v[:, 0:LANES].astype(BF)
            ug_ref[at, :] = v[:, LANES:].astype(BF)
            dg_ref[:, at] = (dot_tn(hid[0], rows[0, q, 1]) + dot_tn(hid[1], rows[1, q, 1])).astype(BF)

    def turn():
        mixt[...] = jnp.zeros_like(mixt)
        pr, pc = iota((2 * RPG, 16 * PER), 0), iota((2 * RPG, 16 * PER), 1)
        second = pr >= RPG
        rest = pr - jnp.where(second, RPG, 0)
        src = div5(rest)
        perm[...] = (pc == src * 16 + (rest - src * CAP) + jnp.where(second, CAP, 0)).astype(BF)
        for cp in weight_moves:
            cp.wait_recv()
        for k in range(8):
            at = slice(k * WIDE, (k + 1) * WIDE)
            dwt[at, :] = dw[:, at].T
            for hf in range(2):
                w4t[hf * WIDE:(hf + 1) * WIDE, at] = w4[at, hf * WIDE:(hf + 1) * WIDE].T

    def tables():
        er = iota((nep, tokn), 0)
        oh0, oh1 = er == r0, er == r1
        ranks = dot((oh0 | oh1).astype(BF), upper)
        aux[0:1, :] = jnp.sum(jnp.where(oh0, ranks, 0.0), axis=0, keepdims=True)
        aux[1:2, :] = jnp.sum(jnp.where(oh1, ranks, 0.0), axis=0, keepdims=True)
        blk8 = 128
        for b in range(nep * 8 // blk8):
            rw = iota((blk8, tokn), 0) + b * blk8
            hit = ((rw >> 3) == r0) | ((rw >> 3) == r1)
            rk = dot(hit.astype(BF), upper)
            s = rw & 7
            p8[pl.ds(b * blk8, blk8), :] = (hit & (rk == s.astype(F32)) & (s < CAP)).astype(BF)
        aux[2:3, :] = w0
        aux[3:4, :] = w1
        aux[4:5, :] = r0.astype(F32)
        aux[5:6, :] = r1.astype(F32)
        aux[6:8, :] = jnp.zeros((2, tokn), F32)

    steps = {"A": gather_out, "B": gather_in, "H": gather_far, "P": first_products, "C": compute, "E": scatter_two, "F": give_back}
    def run(plan):
        for step in plan.split():
            kind, g = step[0], int(step[1:] or 0)
            with jax.named_scope(step):
                if kind == "r":
                    relay(g)
                elif kind == "s":
                    pl.when(z < NZ // 4)(functools.partial(relay, g))
                elif kind == "t":
                    pl.when(z >= NZ // 4)(functools.partial(relay, g))
                elif kind == "G":
                    grads()
                elif kind == "W":
                    turn()
                elif kind == "T":
                    tables()
                else:
                    steps[kind](g)

    early = z < NZ // 2
    pl.when(early)(functools.partial(run, EARLY))
    pl.when(jnp.logical_not(early))(functools.partial(run, LATE))

    for cp in weight_moves:
        cp.wait_send()

    @pl.when(active)
    def _():
        await_bytes(msg.at[:, pl.ds(0, NY - 1), :, pl.ds(0, MSG)], y_send)
        await_bytes(ret.at[pl.ds(0, nep - 1)], rt_send)

    @pl.when(jnp.logical_not(active))
    def _():
        await_bytes(ret, rt_send)

    await_bytes(zbuf.at[pl.ds(0, NZ - 1), :, :, pl.ds(0, MSG)], z_send)
    await_bytes(rows.at[0, pl.ds(0, 3)], ag_send)
    await_bytes(rows.at[0], sib_send)
    await_bytes(obgu, bh_send.at[0])
    await_bytes(ohid, bh_send.at[1])
    await_bytes(sb, rs_send)

    with jax.named_scope("retwait"):
        @pl.when(active)
        def _():
            await_bytes(ret.at[pl.ds(0, nep - 1)], rt_recv)

        @pl.when(jnp.logical_not(active))
        def _():
            await_bytes(ret, rt_recv)


def finish(ret, p8, aux, gg, ug, dg, tg_ref, mg_ref, gg_out, ug_out, dg_out, tg, mg, sem):
    copies = [
        pltpu.make_async_copy(gg, gg_out.at[0], sem.at[0]),
        pltpu.make_async_copy(ug, ug_out.at[0], sem.at[1]),
        pltpu.make_async_copy(dg, dg_out.at[0], sem.at[2]),
    ]
    for cp in copies:
        cp.start()
    nep = ret.shape[0]
    tokn = p8.shape[1]
    back_rows = ret[...].reshape(nep * 8, LANES)
    tg[...] = dot_tn(p8[...], back_rows).astype(BF)
    copies.append(pltpu.make_async_copy(tg, tg_ref, sem.at[3]))
    copies[-1].start()
    sr, sc = iota((nep, nep * 8), 0), iota((nep, nep * 8), 1)
    mixes = dot((sc == sr * 8 + CAP).astype(BF), back_rows).astype(BF)
    lane = iota((LANES, tokn), 0).astype(F32)
    er = iota((nep, tokn), 0).astype(F32)
    done = []
    for k in range(2):
        seen = dot_tn(mixes, (er == aux[4 + k:5 + k, :]).astype(BF))
        rank = aux[k:k + 1, :]
        picked = jnp.where((lane == rank) | (lane == rank + 8.0), seen, 0.0)
        done.append(jnp.sum(picked, axis=0, keepdims=True) / aux[2 + k:3 + k, :])
    mg[...] = jnp.concatenate(done, axis=0).astype(BF)
    copies.append(pltpu.make_async_copy(mg, mg_ref, sem.at[4]))
    copies[-1].start()
    for cp in copies:
        cp.wait()


def solution(mesh):
    nep = NZ * NY

    def on_device(tokens, cotangent, mix_weights, routes, gate_proj, up_proj, down_proj):
        tokn, width = tokens.shape
        ff = gate_proj.shape[2]
        vm = pl.BlockSpec(memory_space=pltpu.VMEM)
        hbm = pl.BlockSpec(memory_space=pltpu.HBM)
        dma = pltpu.SemaphoreType.DMA
        parts = pl.pallas_call(
            kernel,
            out_shape=(
                jax.ShapeDtypeStruct((nep, 8, LANES), BF),
                jax.ShapeDtypeStruct((nep * 8, tokn), BF),
                jax.ShapeDtypeStruct((8, tokn), F32),
                jax.ShapeDtypeStruct((width, ff), BF),
                jax.ShapeDtypeStruct((width, ff), BF),
                jax.ShapeDtypeStruct((ff, width), BF),
            ),
            in_specs=[hbm] * 7,
            out_specs=[vm] * 6,
            scratch_shapes=[
                pltpu.VMEM((2, tokn), jnp.int32),
                pltpu.VMEM((2, tokn), BF),
                pltpu.VMEM((2, tokn, QUAD), BF),
                pltpu.VMEM((NZ, NY, 4, 16, LANES), BF),
                pltpu.VMEM((NZ, HY, 4, 16, LANES), BF),
                pltpu.VMEM((NZ, HY, 4, 16, LANES), BF),
                pltpu.VMEM((2, QUADS, 2, GROUPS * RPG, QUAD), BF),
                pltpu.VMEM((width, 4 * LANES), BF),
                pltpu.VMEM((2 * ff, width), BF),
                pltpu.VMEM((4 * LANES, width), BF),
                pltpu.VMEM((width, 2 * ff), BF),
                pltpu.VMEM((2 * RPG, 16 * PER), BF),
                pltpu.VMEM((2, GROUPS * RPG, WIDE), BF),
                pltpu.VMEM((2, GROUPS * RPG, LANES), BF),
                pltpu.VMEM((GROUPS, RPG, WIDE), BF),
                pltpu.VMEM((GROUPS, RPG, LANES), BF),
                pltpu.VMEM((GROUPS, 8, LANES), F32),
                pltpu.VMEM((GROUPS, RPG, QUAD), F32),
                pltpu.VMEM((GROUPS, RPG, WIDE), F32),
                pltpu.VMEM((GROUPS, 3, 2 * RPG, LANES), F32),
                pltpu.VMEM((GROUPS, 7, TILE, LANES), BF),
                pltpu.VMEM((GROUPS, 7, TILE, LANES), BF),
                pltpu.VMEM((GROUPS, 2, PER, 8, LANES), BF),
                pltpu.SemaphoreType.REGULAR((NZ,)),
                dma((2,)), dma((2,)), dma((3,)), dma((4,)), dma, dma((GROUPS,)), dma, dma((NZ,)),
                dma, dma((4, GROUPS)), dma, dma,
                dma((2,)), dma((2,)), dma, dma((GROUPS, 8)), dma, dma,
            ],
            compiler_params=pltpu.CompilerParams(
                collective_id=0, has_side_effects=True, vmem_limit_bytes=52 * 1024 * 1024),
        )(*(
            pltpu.with_memory_space_constraint(a, pltpu.HBM)
            for a in (tokens, cotangent, routes.T, mix_weights.T, gate_proj, up_proj, down_proj)))
        tg, mg, gg, ug, dg = pl.pallas_call(
            finish,
            out_shape=(
                jax.ShapeDtypeStruct((tokn, LANES), BF),
                jax.ShapeDtypeStruct((2, tokn), BF),
                jax.ShapeDtypeStruct((1, width, ff), BF),
                jax.ShapeDtypeStruct((1, width, ff), BF),
                jax.ShapeDtypeStruct((1, ff, width), BF),
            ),
            in_specs=[vm] * 6,
            out_specs=[hbm] * 5,
            scratch_shapes=[pltpu.VMEM((tokn, LANES), BF), pltpu.VMEM((2, tokn), BF), dma((5,))],
            compiler_params=pltpu.CompilerParams(vmem_limit_bytes=8 * 1024 * 1024),
        )(*parts)
        return tg, mg.T, gg, ug, dg

    in_specs = (
        P("ep", None), P("ep", None), P("ep", None), P("ep", None),
        P("ep", None, "tp"), P("ep", None, "tp"), P("ep", "tp", None),
    )
    out_specs = (
        P("ep", "tp"), P("ep", None), P("ep", None, "tp"), P("ep", None, "tp"), P("ep", "tp", None),
    )
    return jax.shard_map(on_device, mesh=mesh, in_specs=in_specs, out_specs=out_specs, check_vma=False)
```

time: 204 us -> 63.2 us (0.31)
  the two profiles are of different devices: /device:TPU:1 before, /device:TPU:257 now
where the time goes in v2:
time: 63.2 us; the launch traced here: 63.1 us
  Pallas kernels  62.2 us (98%)
  between operations  0.82 us (1%)
    pallas_call x1, Pallas kernels, on_device(): pl.pallas_call(kernel, out_shape=(jax.ShapeDtypeStruct((nep, 8, LANES), B...  61 us

profile of v2, /device:TPU:257, one launch (start us, length us, event | category | flops | bytes accessed | tf_op | source)
XLA Modules:
  0.0 63.1 jit_solution(13884087306306050121)
XLA Ops:
  0.6 61.0 %shard_map.110 = (bf16[64,8,128]{2,1,0:T(8,128)(2,1)S(1)}, bf16[512,128]{1,0:T(8,128)(2,1)S(1)}, f32[8,128]{1,0:T(8,128)S(1)}, bf16[2048,128]{1,0:T(8,128)(2,1)S...) custom-call(bf16[128,2048]{1,0:T(8,128)(2,1)} %tok_hbm.1, bf16[128,2048]{1,0:T(8,128)(2,1)} %cot_hbm.1, ...), custom_call_target="tpu_custom_call" | custom-call | tf_op jit(solution)/shard_map/pallas_call | solution.py:490
  61.7 1.2 %shard_map.111 = (bf16[128,128]{1,0:T(8,128)(2,1)}, bf16[2,128]{1,0:T(2,128)(2,1)}, bf16[1,2048,128]{2,1,0:T(8,128)(2,1)}, bf16[1,2048,128]{2,1,0:T(8,128)(2,1)}, bf16[1,128,2048]{2,1,0:T(8,128)(2,1)}) custom-call(bf16[64,8,128]{2,1,0:T(8,128)(2,1)S(1)} %get-tuple-element.16.ret, bf16[512,128]{1,0:T(8,128)(2,1)S(1)} %get-tuple-element.17.p8, ...), custom_call_target="tpu_custom_call" | custom-call | tf_op jit(solution)/shard_map/pallas_call | solution.py:536

commit v3 on v2

--- a/solution.py
+++ b/solution.py
@@ -20,13 +20,13 @@
 PER = ZB * HY
 RPG = PER * CAP
 TILE = 2 * RPG + 8
+SENT = 2 * RPG + 2
 CUT = 40
 WIDE = 2 * LANES
 QUADS = 4
 QUAD = 4 * LANES
-DIRECT = ()
-EARLY = "W r0 r1 r2 s3 A0 A1 B0 t3 B1 P0 A2 H0 C0 A3 P1 B2 H1 P2 E0 B3 P3 H2 C2 F0 C1 H3 C3 E2 E1 E3 F2 F1 F3 T G"
-LATE = "W r0 A0 r1 r2 r3 B0 P0 A3 A1 H0 C0 A2 B1 P1 E0 H1 C1 B2 B3 F0 P2 E1 H2 C2 P3 H3 C3 F1 E2 E3 F2 F3 T G"
+EARLY = "W r0 r1 r2 s3 A0 A1 t3 f0 f1 B0 f2 f3 H0 Q0 C0 A2 E0 A3 B1 Q1 H1 C1 H2 B2 Q2 C2 F0 H3 P3 B3 C3 E1 E3 E2 T G F1 F3 F2"
+LATE = "W r0 A0 r1 f0 f1 A1 r2 r3 B0 Q0 H0 C0 A2 H1 f2 E0 f3 B1 P1 C1 H3 B2 H2 A3 P2 C2 F0 E1 P3 E2 B3 F1 C3 F2 E3 F3 T G"
 
 
 def iota(shape, dim):
@@ -61,9 +61,10 @@
     t = lax.axis_index("tp")
     z, y = e // NY, e % NY
     x, c = t // 2, t % 2
-    tokn = share.shape[1]
+    tokn = share.shape[2]
     nep = NZ * NY
-    active = y % 2 == c
+    mine_y = 1 - c
+    active = y // HY == mine_y
 
     def chip(d):
         return lax.rem(x + d + NX, NX)
@@ -83,22 +84,22 @@
     def await_bytes(ref, sem):
         pltpu.make_async_copy(ref, ref, sem).wait()
 
-    col = pl.multiple_of(quad(0) * QUAD, QUAD)
+    cols = [pl.ds(pl.multiple_of(quad(d) * QUAD, QUAD), QUAD) for d in (0, 2)]
     table_copies = [
         pltpu.make_async_copy(routes_hbm, routes_ref, t_sem.at[0]),
         pltpu.make_async_copy(mix_hbm, mix_ref, t_sem.at[1]),
     ]
     share_copies = [
-        pltpu.make_async_copy(tok_hbm.at[:, pl.ds(col, QUAD)], share.at[0], sh_sem.at[0]),
-        pltpu.make_async_copy(cot_hbm.at[:, pl.ds(col, QUAD)], share.at[1], sh_sem.at[1]),
+        pltpu.make_async_copy(ref.at[:, cols[part]], share.at[part, i], sh_sem)
+        for part in range(2) for i, ref in enumerate((tok_hbm, cot_hbm))
     ]
     lane = pl.multiple_of(c * WIDE, WIDE)
     ours = w4.at[:, pl.ds(lane, WIDE)]
     downs = dw.at[pl.ds(pl.multiple_of(c * LANES, LANES), LANES)]
     weight_copies = [
-        pltpu.make_async_copy(gate_hbm.at[0], w4.at[:, pl.ds(lane, LANES)], w_sem.at[0]),
-        pltpu.make_async_copy(up_hbm.at[0], w4.at[:, pl.ds(pl.multiple_of(lane + LANES, LANES), LANES)], w_sem.at[1]),
-        pltpu.make_async_copy(down_hbm.at[0], downs, w_sem.at[2]),
+        pltpu.make_async_copy(gate_hbm.at[0], w4.at[:, pl.ds(lane, LANES)], w_sem),
+        pltpu.make_async_copy(up_hbm.at[0], w4.at[:, pl.ds(pl.multiple_of(lane + LANES, LANES), LANES)], w_sem),
+        pltpu.make_async_copy(down_hbm.at[0], downs, w_sem),
     ]
     weight_moves = [
         remote(ours, ours, x_sem.at[0], x_sem.at[1], sib),
@@ -131,14 +132,14 @@
     w0, w1 = w[0:1, :], w[1:2, :]
     upper = (iota((tokn, tokn), 0) < iota((tokn, tokn), 1)).astype(BF)
     with jax.named_scope("share"):
-        for cp in share_copies:
-            cp.wait()
+        await_bytes(share, sh_sem)
 
     @pl.when(active)
     def _():
-        both = share[...].reshape(2 * tokn, QUAD)
+        both = jnp.concatenate([share[part].reshape(2 * tokn, QUAD) for part in range(2)], axis=1)
         blk = ZB * NY * 16
-        for b in range(GROUPS):
+
+        def fill(b):
             rw = iota((blk, tokn), 0) + b * blk
             ex = rw >> 4
             q = rw & 15
@@ -150,94 +151,118 @@
             two = jnp.where(hit & (rk == (q - CAP).astype(F32)) & (q >= CAP), wt, 0.0)
             sel = jnp.concatenate([one.astype(BF), two.astype(BF)], axis=1)
             v = dot(sel, both).astype(BF)
-            for ch in range(4):
-                msg[pl.ds(b * ZB, ZB), :, ch] = v[:, ch * LANES:(ch + 1) * LANES].reshape(ZB, NY, 16, LANES)
+            for part in range(2):
+                for ch in range(4):
+                    at = part * QUAD + ch * LANES
+                    msg[part, pl.ds(b * ZB, ZB), :, ch] = v[:, at:at + LANES].reshape(ZB, NY, 16, LANES)
+
+        def tell(b, part):
+            zz = pl.ds(b * ZB, ZB)
             for d in (4, 3, 5, 2, 6, 1, 7):
                 yd = lax.rem(y + d, NY)
                 remote(
-                    msg.at[pl.ds(b * ZB, ZB), yd, :, pl.ds(0, MSG)],
-                    ybuf.at[pl.ds(b * ZB, ZB), y // 2, :, pl.ds(0, MSG)],
-                    y_send, y_recv.at[b], (z * NY + yd, t)).start()
-            ybuf[pl.ds(b * ZB, ZB), y // 2] = msg[pl.ds(b * ZB, ZB), y]
-
-    for cp in weight_copies:
-        cp.wait()
+                    msg.at[part, zz, yd, :, pl.ds(0, MSG)], ybuf.at[part, zz, y % HY, :, pl.ds(0, MSG)],
+                    y_send, y_recv.at[part, b], (z * NY + yd, t)).start()
+            ybuf[part, zz, y % HY] = msg[part, zz, y]
+
+        for b in (0, 1):
+            fill(b)
+            tell(b, 0)
+
+        @pl.when(z >= NZ // 2)
+        def _():
+            for b in (0, 1):
+                tell(b, 1)
+
+        for b in (2, 3):
+            fill(b)
+            tell(b, 0)
+
+        @pl.when(z < NZ // 2)
+        def _():
+            for b in (0, 1):
+                tell(b, 1)
+
+        for b in (2, 3):
+            tell(b, 1)
+
+    await_bytes(w4.at[:, pl.ds(0, 3 * LANES)], w_sem)
     for cp in weight_moves:
         cp.start()
 
-    def relay(b):
-        with jax.named_scope(f"ywait{b}"):
+    def relay(b, part=0):
+        with jax.named_scope(f"ywait{b}{'f' if part else ''}"):
+            zz = pl.ds(b * ZB, ZB)
+
             @pl.when(active)
             def _():
-                await_bytes(ybuf.at[pl.ds(b * ZB, ZB), pl.ds(0, HY - 1), :, pl.ds(0, MSG)], y_recv.at[b])
+                await_bytes(ybuf.at[part, zz, pl.ds(0, HY - 1), :, pl.ds(0, MSG)], y_recv.at[part, b])
 
             @pl.when(jnp.logical_not(active))
             def _():
-                await_bytes(ybuf.at[pl.ds(b * ZB, ZB), :, :, pl.ds(0, MSG)], y_recv.at[b])
+                await_bytes(ybuf.at[part, zz, :, :, pl.ds(0, MSG)], y_recv.at[part, b])
         for zd in range(b * ZB, (b + 1) * ZB):
             @pl.when(zd == z)
             def _():
-                zbuf[zd] = ybuf[zd]
-
-            @pl.when(zd > z)
-            def _():
-                with jax.named_scope(f"ready{zd}"):
-                    pl.semaphore_wait(ready.at[zd], 1)
+                zbuf[part, zd] = ybuf[part, zd]
+
+            if part == 0:
+                @pl.when(zd > z)
+                def _():
+                    with jax.named_scope(f"ready{zd}"):
+                        pl.semaphore_wait(ready.at[zd], 1)
 
             @pl.when(zd != z)
             def _():
                 remote(
-                    ybuf.at[zd, :, :, pl.ds(0, MSG)], zbuf.at[z, :, :, pl.ds(0, MSG)],
-                    z_send, z_recv.at[z], (zd * NY + y, t)).start()
+                    ybuf.at[part, zd, :, :, pl.ds(0, MSG)], zbuf.at[part, z, :, :, pl.ds(0, MSG)],
+                    z_send, z_recv.at[part, z // ZB], (zd * NY + y, t)).start()
 
     def unit(d, g):
         return rows.at[c, quad(d), :, pl.ds(g * RPG, RPG)]
-
-    def half(d, g, i):
-        return rows.at[c, quad(d), i, pl.ds(g * RPG, RPG)]
 
     def to_sib(d, g):
         u = unit(d, g)
         remote(u, u, sib_send, sib_recv, sib).start()
 
-    def gather_out(g):
-        for zs in range(g * ZB, (g + 1) * ZB):
-            @pl.when(zs != z)
+    def landed(g, part):
+        with jax.named_scope(f"zwait{g}{'f' if part else ''}"):
+            @pl.when(z // ZB == g)
             def _():
-                with jax.named_scope(f"zwait{zs}"):
-                    await_bytes(zbuf.at[zs, :, :, pl.ds(0, MSG)], z_recv.at[zs])
+                await_bytes(zbuf.at[part, pl.ds(0, ZB - 1), :, :, pl.ds(0, MSG)], z_recv.at[part, g])
+
+            @pl.when(z // ZB != g)
+            def _():
+                await_bytes(zbuf.at[part, pl.ds(0, ZB), :, :, pl.ds(0, MSG)], z_recv.at[part, g])
         got = jnp.concatenate(
-            [zbuf[pl.ds(g * ZB, ZB), :, ch].reshape(PER * 16, LANES) for ch in range(4)], axis=1)
+            [zbuf[part, pl.ds(g * ZB, ZB), :, ch].reshape(PER * 16, LANES) for ch in range(4)], axis=1)
         got = jnp.where((iota(got.shape, 0) & 15) < MSG, got, jnp.zeros_like(got))
         v = dot(perm[...], got)
-        rows[c, quad(0), 0, g * RPG:(g + 1) * RPG] = v[0:RPG].astype(BF)
-        rows[c, quad(0), 1, g * RPG:(g + 1) * RPG] = v[RPG:].astype(BF)
+        q = quad(2 * part)
+        rows[c, q, 0, g * RPG:(g + 1) * RPG] = v[0:RPG].astype(BF)
+        rows[c, q, 1, g * RPG:(g + 1) * RPG] = v[RPG:].astype(BF)
+
+    def gather_out(g):
+        landed(g, 0)
         u = unit(0, g)
-        remote(u, u, ag_send, ag_recv.at[0, g], along_x(1)).start()
-        remote(u, u, ag_send, ag_recv.at[1, g], along_x(-1)).start()
-        if g in DIRECT:
-            for i, d in ((0, 2), (1, -2)):
-                h = half(0, g, i)
-                remote(h, h, ag_send, ag_recv.at[2 + i, g], along_x(d)).start()
+        remote(u, u, ag_send, ag_recv.at[g], along_x(1)).start()
+        remote(u, u, ag_send, ag_recv.at[g], along_x(-1)).start()
         to_sib(0, g)
 
+    def gather_far(g):
+        landed(g, 1)
+        to_sib(2, g)
+
     def gather_in(g):
-        for i, d in ((0, -1), (1, 1)):
-            await_bytes(unit(d, g), ag_recv.at[i, g])
-            if g not in DIRECT:
-                h = half(d, g, i)
-                remote(h, h, ag_send, ag_recv.at[2 + i, g], along_x(-d)).start()
-            to_sib(d, g)
-
-    def gather_far(g):
-        for i in range(2):
-            await_bytes(half(2, g, i), ag_recv.at[2 + i, g])
-        to_sib(2, g)
-
-    def send_part(g, i, to):
-        remote(sb.at[g, i], rb.at[g, i], rs_send, rs_recv.at[g, i], along_x(to)).start()
-
-    near, past = pl.ds(0, CUT), pl.ds(CUT, TILE - CUT)
+        await_bytes(rows.at[c, pl.ds(0, 2), :, pl.ds(g * RPG, RPG)], ag_recv.at[g])
+        to_sib(-1, g)
+        to_sib(1, g)
+
+    def send_part(g, first, count, phase, to):
+        at = (g, pl.ds(first, count), pl.ds(0, SENT))
+        remote(sb.at[at], rb.at[at], rs_send, rs_recv.at[g, phase], along_x(to)).start()
+
+    near, past = pl.ds(0, CUT), pl.ds(CUT, SENT - CUT)
 
     def products(g, d):
         at = pl.ds(g * RPG, RPG)
@@ -245,16 +270,18 @@
         features = pl.ds(pl.multiple_of(q * QUAD, QUAD), QUAD)
         return dot(rows[c, q, 0, at], w4[features, :]), dot(rows[c, q, 1, at], dwt[features, :])
 
-    def first_products(g):
-        each = [products(g, d) for d in (0, -1, 1)]
-        pre[g] = each[0][0] + each[1][0] + each[2][0]
-        back[g] = each[0][1] + each[1][1] + each[2][1]
-
-    def compute(g):
+    def first_products(g, ds):
+        each = [products(g, d) for d in ds]
+        pre[g] = sum((a for a, _ in each[1:]), each[0][0])
+        back[g] = sum((b for _, b in each[1:]), each[0][1])
+
+    def compute(g, ds):
         at = pl.ds(g * RPG, RPG)
-        pgu, bh = products(g, 2)
-        pgu = pgu + pre[g]
-        bh = bh + back[g]
+        pgu, bh = pre[g], back[g]
+        for d in ds:
+            a, b = products(g, d)
+            pgu = pgu + a
+            bh = bh + b
         pg = jnp.concatenate([pgu[:, 0:LANES], pgu[:, WIDE:WIDE + LANES]], axis=1)
         pu = jnp.concatenate([pgu[:, LANES:WIDE], pgu[:, WIDE + LANES:]], axis=1)
         sig = jax.nn.sigmoid(pg)
@@ -274,21 +301,27 @@
         row = iota((8, RPG), 0)
         mixt[g, :, 0:RPG] = jnp.where(row == 0, shi, jnp.where(row == 1, sums - shi, 0.0))
         tile = mixt[g].astype(BF)
-        for d, i, to in ((3, 0, 1), (5, 1, -1), (4, 4, 0), (1, 2, 1), (7, 3, -1), (2, 0, None), (6, 1, None), (0, 2, None)):
+        def part(d):
             cols = pl.ds(pl.multiple_of(chip(d) * WIDE, WIDE), WIDE)
-            v = dot(b4, w4t[:, cols])
-            if to is None:
-                pown[g, i, 0:RPG] = v[:, 0:LANES]
-                pown[g, i, RPG:2 * RPG] = v[:, LANES:]
-            else:
-                sb[g, i, 0:RPG] = v[:, 0:LANES].astype(BF)
-                sb[g, i, RPG:2 * RPG] = v[:, LANES:].astype(BF)
-                sb[g, i, 2 * RPG:] = tile
-                if to:
-                    send_part(g, i, to)
-                else:
-                    remote(sb.at[g, 4, near], rb.at[g, 4, near], rs_send, rs_recv.at[g, 4], along_x(2)).start()
-                    remote(sb.at[g, 4, past], rb.at[g, 4, past], rs_send, rs_recv.at[g, 7], along_x(-2)).start()
+            return dot(b4, w4t[:, cols])
+
+        def stored(d, i):
+            v = part(d)
+            sb[g, i, 0:RPG] = v[:, 0:LANES].astype(BF)
+            sb[g, i, RPG:2 * RPG] = v[:, LANES:].astype(BF)
+            sb[g, i, 2 * RPG:] = tile
+
+        stored(4, 4)
+        for rows_, to in ((near, 2), (past, -2)):
+            remote(sb.at[g, 4, rows_], rb.at[g, 4, rows_], rs_send, rs_recv.at[g, 0], along_x(to)).start()
+        for d, i, to in ((3, 0, 1), (5, 2, -1)):
+            stored(d, i)
+            stored(to % NX, i + 1)
+            send_part(g, i, 2, 0, to)
+        for d, i in ((2, 0), (6, 1), (0, 2)):
+            v = part(d)
+            pown[g, i, 0:RPG] = v[:, 0:LANES]
+            pown[g, i, RPG:2 * RPG] = v[:, LANES:]
         first = c == 0
         bgu[c, at] = jnp.where(first, b0.astype(F32), b1.astype(F32)).astype(BF)
         obgu[g] = jnp.where(first, b1.astype(F32), b0.astype(F32)).astype(BF)
@@ -302,23 +335,20 @@
         return jnp.concatenate([pown[g, i], mixt[g]], axis=0)
 
     def scatter_two(g):
-        await_bytes(rb.at[g, 0], rs_recv.at[g, 0])
-        await_bytes(rb.at[g, 4, near], rs_recv.at[g, 4])
+        await_bytes(rb.at[g, pl.ds(0, 5), pl.ds(0, SENT)], rs_recv.at[g, 0])
         v = chunk(g, 0) + rb[g, 0].astype(F32)
         sb[g, 5, 0:CUT] = (v[0:CUT] + rb[g, 4, 0:CUT].astype(F32)).astype(BF)
         sb[g, 5, CUT:] = v[CUT:].astype(BF)
-        send_part(g, 5, 2)
-        await_bytes(rb.at[g, 1], rs_recv.at[g, 1])
-        await_bytes(rb.at[g, 4, past], rs_recv.at[g, 7])
-        v = chunk(g, 1) + rb[g, 1].astype(F32)
+        send_part(g, 5, 1, 1, 2)
+        v = chunk(g, 1) + rb[g, 2].astype(F32)
         sb[g, 6, 0:CUT] = v[0:CUT].astype(BF)
         sb[g, 6, CUT:] = (v[CUT:] + rb[g, 4, CUT:].astype(F32)).astype(BF)
-        send_part(g, 6, -2)
+        send_part(g, 6, 1, 1, -2)
 
     def give_back(g):
+        await_bytes(rb.at[g, pl.ds(0, 2), pl.ds(0, SENT)], rs_recv.at[g, 1])
         v = chunk(g, 2)
-        for i in (2, 3, 5, 6):
-            await_bytes(rb.at[g, i], rs_recv.at[g, i])
+        for i in (1, 3, 5, 6):
             v = v + rb[g, i].astype(F32)
         sums = v[2 * RPG:2 * RPG + 1] + v[2 * RPG + 1:2 * RPG + 2]
         mhi = sums.astype(BF).astype(F32)
@@ -337,7 +367,7 @@
         m = m + dot(jnp.where(take, mlo, 0.0).astype(BF), (bc == slot_r + 8).astype(BF))
         out[g] = m.astype(BF).reshape(2, PER, 8, LANES)
         for j in range(PER):
-            i = (g * ZB + j // HY) * NY + 2 * (j % HY) + c
+            i = (g * ZB + j // HY) * NY + mine_y * HY + j % HY
             for hf in range(2):
                 here_ = (i == e) & (c == hf)
 
@@ -394,17 +424,26 @@
         aux[5:6, :] = r1.astype(F32)
         aux[6:8, :] = jnp.zeros((2, tokn), F32)
 
-    steps = {"A": gather_out, "B": gather_in, "H": gather_far, "P": first_products, "C": compute, "E": scatter_two, "F": give_back}
+    steps = {"A": gather_out, "B": gather_in, "H": gather_far, "E": scatter_two, "F": give_back}
     def run(plan):
+        left = {}
         for step in plan.split():
             kind, g = step[0], int(step[1:] or 0)
             with jax.named_scope(step):
                 if kind == "r":
                     relay(g)
-                elif kind == "s":
-                    pl.when(z < NZ // 4)(functools.partial(relay, g))
-                elif kind == "t":
-                    pl.when(z >= NZ // 4)(functools.partial(relay, g))
+                elif kind == "f":
+                    relay(g, 1)
+                elif kind in "st":
+                    pl.when((z < NZ // 4) == (kind == "s"))(functools.partial(relay, g))
+                elif kind == "P":
+                    first_products(g, (0, 2))
+                    left[g] = (-1, 1)
+                elif kind == "Q":
+                    first_products(g, (0, -1, 1))
+                    left[g] = (2,)
+                elif kind == "C":
+                    compute(g, left[g])
                 elif kind == "G":
                     grads()
                 elif kind == "W":
@@ -423,19 +462,19 @@
 
     @pl.when(active)
     def _():
-        await_bytes(msg.at[:, pl.ds(0, NY - 1), :, pl.ds(0, MSG)], y_send)
+        await_bytes(msg.at[:, :, pl.ds(0, NY - 1), :, pl.ds(0, MSG)], y_send)
         await_bytes(ret.at[pl.ds(0, nep - 1)], rt_send)
 
     @pl.when(jnp.logical_not(active))
     def _():
         await_bytes(ret, rt_send)
 
-    await_bytes(zbuf.at[pl.ds(0, NZ - 1), :, :, pl.ds(0, MSG)], z_send)
-    await_bytes(rows.at[0, pl.ds(0, 3)], ag_send)
+    await_bytes(zbuf.at[:, pl.ds(0, NZ - 1), :, :, pl.ds(0, MSG)], z_send)
+    await_bytes(rows.at[0, pl.ds(0, 2)], ag_send)
     await_bytes(rows.at[0], sib_send)
     await_bytes(obgu, bh_send.at[0])
     await_bytes(ohid, bh_send.at[1])
-    await_bytes(sb, rs_send)
+    await_bytes(sb.at[:, :, pl.ds(0, SENT)], rs_send)
 
     with jax.named_scope("retwait"):
         @pl.when(active)
@@ -502,10 +541,10 @@
             scratch_shapes=[
                 pltpu.VMEM((2, tokn), jnp.int32),
                 pltpu.VMEM((2, tokn), BF),
-                pltpu.VMEM((2, tokn, QUAD), BF),
-                pltpu.VMEM((NZ, NY, 4, 16, LANES), BF),
-                pltpu.VMEM((NZ, HY, 4, 16, LANES), BF),
-                pltpu.VMEM((NZ, HY, 4, 16, LANES), BF),
+                pltpu.VMEM((2, 2, tokn, QUAD), BF),
+                pltpu.VMEM((2, NZ, NY, 4, 16, LANES), BF),
+                pltpu.VMEM((2, NZ, HY, 4, 16, LANES), BF),
+                pltpu.VMEM((2, NZ, HY, 4, 16, LANES), BF),
                 pltpu.VMEM((2, QUADS, 2, GROUPS * RPG, QUAD), BF),
                 pltpu.VMEM((width, 4 * LANES), BF),
                 pltpu.VMEM((2 * ff, width), BF),
@@ -524,9 +563,9 @@
                 pltpu.VMEM((GROUPS, 7, TILE, LANES), BF),
                 pltpu.VMEM((GROUPS, 2, PER, 8, LANES), BF),
                 pltpu.SemaphoreType.REGULAR((NZ,)),
-                dma((2,)), dma((2,)), dma((3,)), dma((4,)), dma, dma((GROUPS,)), dma, dma((NZ,)),
-                dma, dma((4, GROUPS)), dma, dma,
-                dma((2,)), dma((2,)), dma, dma((GROUPS, 8)), dma, dma,
+                dma((2,)), dma, dma, dma((4,)), dma, dma((2, GROUPS)), dma, dma((2, GROUPS)),
+                dma, dma((GROUPS,)), dma, dma,
+                dma((2,)), dma((2,)), dma, dma((GROUPS, 2)), dma, dma,
             ],
             compiler_params=pltpu.CompilerParams(
                 collective_id=0, has_side_effects=True, vmem_limit_bytes=52 * 1024 * 1024),

time: 63.2 us -> 58.6 us (0.927)
  the two profiles are of different devices: /device:TPU:257 before, /device:TPU:1 now
where the time goes in v3:
time: 58.6 us; the launch traced here: 58.2 us
  Pallas kernels  57.4 us (98%)
  between operations  0.82 us (1%)
    pallas_call x1, Pallas kernels, on_device(): pl.pallas_call(kernel, out_shape=(jax.ShapeDtypeStruct((nep, 8, LANES), B...  56.2 us
    pallas_call x1, Pallas kernels, on_device(): pl.pallas_call(finish, out_shape=(jax.ShapeDtypeStruct((tokn, LANES), BF)...  1.19 us

profile of v3, /device:TPU:1, one launch (start us, length us, event | category | flops | bytes accessed | tf_op | source)
XLA Modules:
  0.0 58.2 jit_solution(470533614580904353)
XLA Ops:
  0.6 56.2 %shard_map.110 = (bf16[64,8,128]{2,1,0:T(8,128)(2,1)S(1)}, bf16[512,128]{1,0:T(8,128)(2,1)S(1)}, f32[8,128]{1,0:T(8,128)S(1)}, bf16[2048,128]{1,0:T(8,128)(2,1)S...) custom-call(bf16[128,2048]{1,0:T(8,128)(2,1)} %tok_hbm.1, bf16[128,2048]{1,0:T(8,128)(2,1)} %cot_hbm.1, ...), custom_call_target="tpu_custom_call" | custom-call | tf_op jit(solution)/shard_map/pallas_call | solution.py:529
  56.8 1.2 %shard_map.111 = (bf16[128,128]{1,0:T(8,128)(2,1)}, bf16[2,128]{1,0:T(2,128)(2,1)}, bf16[1,2048,128]{2,1,0:T(8,128)(2,1)}, bf16[1,2048,128]{2,1,0:T(8,128)(2,1)}, bf16[1,128,2048]{2,1,0:T(8,128)(2,1)}) custom-call(bf16[64,8,128]{2,1,0:T(8,128)(2,1)S(1)} %get-tuple-element.16.ret, bf16[512,128]{1,0:T(8,128)(2,1)S(1)} %get-tuple-element.17.p8, ...), custom_call_target="tpu_custom_call" | custom-call | tf_op jit(solution)/shard_map/pallas_call | solution.py:575

commit v4 on v3

--- a/solution.py
+++ b/solution.py
@@ -25,8 +25,16 @@
 WIDE = 2 * LANES
 QUADS = 4
 QUAD = 4 * LANES
-EARLY = "W r0 r1 r2 s3 A0 A1 t3 f0 f1 B0 f2 f3 H0 Q0 C0 A2 E0 A3 B1 Q1 H1 C1 H2 B2 Q2 C2 F0 H3 P3 B3 C3 E1 E3 E2 T G F1 F3 F2"
-LATE = "W r0 A0 r1 f0 f1 A1 r2 r3 B0 Q0 H0 C0 A2 H1 f2 E0 f3 B1 P1 C1 H3 B2 H2 A3 P2 C2 F0 E1 P3 E2 B3 F1 C3 F2 E3 F3 T G"
+EARLY = (
+    "W r0 r1 D", "r2 s3 A0 A1", "t3 f0 f1 B0", "f2 f3 H0 Q0", "C0 A2 B1 H1",
+    "P1 C1 A3 E0", "H2 B2 P2 C2", "H3 P3 B3 C3", "F0 E1 E2 E3", "T G F1 F2",
+    "F3",
+)
+LATE = (
+    "W r0 A0 r1", "f0 f1 a1 r2", "r3 B0 z1 Q0", "H0 C0 B1 H1", "P1 C1 A2 f2",
+    "f3 E0 B2 y0", "H2 A3 P2 x0", "E1 C2 H3 P3", "B3 F1 C3 E2", "F2 E3 F3 T",
+    "G",
+)
 
 
 def iota(shape, dim):
@@ -54,7 +62,7 @@
     ret, p8, aux, gg_ref, ug_ref, dg_ref,
     routes_ref, mix_ref, share, msg, ybuf, zbuf, rows, w4, dw, w4t, dwt, perm, bgu, hid, obgu, ohid, mixt,
     pre, back, pown, sb, rb, out,
-    ready, t_sem, sh_sem, w_sem, x_sem, y_send, y_recv, z_send, z_recv, ag_send, ag_recv, sib_send, sib_recv,
+    ready, late, t_sem, sh_sem, w_sem, x_sem, y_send, y_recv, z_send, z_recv, ag_send, ag_recv, sib_send, sib_recv,
     bh_send, bh_recv, rs_send, rs_recv, rt_send, rt_recv,
 ):
     e = lax.axis_index("ep")
@@ -106,19 +114,30 @@
         remote(downs, downs, x_sem.at[2], x_sem.at[3], sib),
     ]
     barrier = pltpu.get_barrier_semaphore()
-    for d in (4, 3, 5, 2, 6, 1, 7):
-        pl.semaphore_signal(barrier, inc=1, device_id=(z * NY + lax.rem(y + d, NY), t), device_id_type=MESH)
+    column = (z == 0) & (t == 0)
+    latecomer = column & (y == 0)
+
+    @pl.when(jnp.logical_not(latecomer))
+    def _():
+        for d in (4, 3, 5, 2, 6, 1, 7):
+            pl.semaphore_signal(barrier, inc=1, device_id=(z * NY + lax.rem(y + d, NY), t), device_id_type=MESH)
+
     for d in (2, -2, 1, -1):
         pl.semaphore_signal(barrier, inc=1, device_id=along_x(d), device_id_type=MESH)
     pl.semaphore_signal(barrier, inc=1, device_id=sib, device_id_type=MESH)
     for cp in table_copies + share_copies + weight_copies:
         cp.start()
     with jax.named_scope("barrier"):
-        pl.semaphore_wait(barrier, 12 + jnp.where(z > 0, 1, 0))
+        pl.semaphore_wait(barrier, 12 + jnp.where(z > 0, 1, 0) - jnp.where(column & (y > 0), 1, 0))
 
     @pl.when(z < NZ - 1)
     def _():
         pl.semaphore_signal(barrier, inc=1, device_id=(e + NY, t), device_id_type=MESH)
+
+    @pl.when(latecomer)
+    def _():
+        for yy in range(HY, NY):
+            pl.semaphore_signal(late, inc=1, device_id=(yy, t), device_id_type=MESH)
 
     for zz in range(NZ - 1):
         @pl.when(zz < z)
@@ -133,6 +152,18 @@
     upper = (iota((tokn, tokn), 0) < iota((tokn, tokn), 1)).astype(BF)
     with jax.named_scope("share"):
         await_bytes(share, sh_sem)
+
+    def tell_one(b, part, yd):
+        zz = pl.ds(b * ZB, ZB)
+        remote(
+            msg.at[part, zz, yd, :, pl.ds(0, MSG)], ybuf.at[part, zz, y % HY, :, pl.ds(0, MSG)],
+            y_send, y_recv.at[part, b], (z * NY + yd, t)).start()
+
+    def tell_latecomer():
+        pl.semaphore_wait(late, 1)
+        for part in range(2):
+            for b in range(GROUPS):
+                tell_one(b, part, 0)
 
     @pl.when(active)
     def _():
@@ -160,9 +191,7 @@
             zz = pl.ds(b * ZB, ZB)
             for d in (4, 3, 5, 2, 6, 1, 7):
                 yd = lax.rem(y + d, NY)
-                remote(
-                    msg.at[part, zz, yd, :, pl.ds(0, MSG)], ybuf.at[part, zz, y % HY, :, pl.ds(0, MSG)],
-                    y_send, y_recv.at[part, b], (z * NY + yd, t)).start()
+                pl.when(jnp.logical_not(column & (yd == 0)))(functools.partial(tell_one, b, part, yd))
             ybuf[part, zz, y % HY] = msg[part, zz, y]
 
         for b in (0, 1):
@@ -427,7 +456,7 @@
     steps = {"A": gather_out, "B": gather_in, "H": gather_far, "E": scatter_two, "F": give_back}
     def run(plan):
         left = {}
-        for step in plan.split():
+        for step in " ".join(plan).split():
             kind, g = step[0], int(step[1:] or 0)
             with jax.named_scope(step):
                 if kind == "r":
@@ -436,6 +465,12 @@
                     relay(g, 1)
                 elif kind in "st":
                     pl.when((z < NZ // 4) == (kind == "s"))(functools.partial(relay, g))
+                elif kind in "az":
+                    pl.when(c == int(kind == "z"))(functools.partial(gather_out, g))
+                elif kind == "D":
+                    pl.when(column & active)(tell_latecomer)
+                elif kind in "xy":
+                    pl.when(c == int(kind == "y"))(functools.partial(give_back, g))
                 elif kind == "P":
                     first_products(g, (0, 2))
                     left[g] = (-1, 1)
@@ -563,6 +598,7 @@
                 pltpu.VMEM((GROUPS, 7, TILE, LANES), BF),
                 pltpu.VMEM((GROUPS, 2, PER, 8, LANES), BF),
                 pltpu.SemaphoreType.REGULAR((NZ,)),
+                pltpu.SemaphoreType.REGULAR,
                 dma((2,)), dma, dma, dma((4,)), dma, dma((2, GROUPS)), dma, dma((2, GROUPS)),
                 dma, dma((GROUPS,)), dma, dma,
                 dma((2,)), dma((2,)), dma, dma((GROUPS, 2)), dma, dma,

time: 58.6 us -> 57.4 us (0.980)
  the two profiles are of different devices: /device:TPU:1 before, /device:TPU:257 now
where the time goes in v4:
time: 57.4 us; the launch traced here: 57.2 us
  Pallas kernels  56.4 us (98%)
  between operations  0.82 us (1%)
    pallas_call x1, Pallas kernels, on_device(): pl.pallas_call(kernel, out_shape=(jax.ShapeDtypeStruct((nep, 8, LANES), B...  55.2 us
    pallas_call x1, Pallas kernels, on_device(): pl.pallas_call(finish, out_shape=(jax.ShapeDtypeStruct((tokn, LANES), BF)...  1.19 us

profile of v4, /device:TPU:257, one launch (start us, length us, event | category | flops | bytes accessed | tf_op | source)
XLA Modules:
  0.0 57.2 jit_solution(17781539609273091181)
XLA Ops:
  0.6 55.2 %shard_map.110 = (bf16[64,8,128]{2,1,0:T(8,128)(2,1)S(1)}, bf16[512,128]{1,0:T(8,128)(2,1)S(1)}, f32[8,128]{1,0:T(8,128)S(1)}, bf16[2048,128]{1,0:T(8,128)(2,1)S...) custom-call(bf16[128,2048]{1,0:T(8,128)(2,1)} %tok_hbm.1, bf16[128,2048]{1,0:T(8,128)(2,1)} %cot_hbm.1, ...), custom_call_target="tpu_custom_call" | custom-call | tf_op jit(solution)/shard_map/pallas_call | solution.py:564
  55.8 1.2 %shard_map.111 = (bf16[128,128]{1,0:T(8,128)(2,1)}, bf16[2,128]{1,0:T(2,128)(2,1)}, bf16[1,2048,128]{2,1,0:T(8,128)(2,1)}, bf16[1,2048,128]{2,1,0:T(8,128)(2,1)}, bf16[1,128,2048]{2,1,0:T(8,128)(2,1)}) custom-call(bf16[64,8,128]{2,1,0:T(8,128)(2,1)S(1)} %get-tuple-element.16.ret, bf16[512,128]{1,0:T(8,128)(2,1)S(1)} %get-tuple-element.17.p8, ...), custom_call_target="tpu_custom_call" | custom-call | tf_op jit(solution)/shard_map/pallas_call | solution.py:611

commit v5 on v4

--- a/solution.py
+++ b/solution.py
@@ -32,7 +32,7 @@
 )
 LATE = (
     "W r0 A0 r1", "f0 f1 a1 r2", "r3 B0 z1 Q0", "H0 C0 B1 H1", "P1 C1 A2 f2",
-    "f3 E0 B2 y0", "H2 A3 P2 x0", "E1 C2 H3 P3", "B3 F1 C3 E2", "F2 E3 F3 T",
+    "f3 E0 A3 E1", "y0 H2 B2 P2", "x0 C2 H3 P3", "F1 B3 C3 E2", "E3 F2 F3 T",
     "G",
 )
 

time: 57.4 us -> 55.6 us (0.969)
  the two profiles are of different devices: /device:TPU:257 before, /device:TPU:1 now
where the time goes in v5:
time: 55.6 us; the launch traced here: 55.5 us
  Pallas kernels  54.6 us (98%)
  between operations  0.82 us (1%)
    pallas_call x1, Pallas kernels, on_device(): pl.pallas_call(kernel, out_shape=(jax.ShapeDtypeStruct((nep, 8, LANES), B...  53.5 us
    pallas_call x1, Pallas kernels, on_device(): pl.pallas_call(finish, out_shape=(jax.ShapeDtypeStruct((tokn, LANES), BF)...  1.19 us

profile of v5, /device:TPU:1, one launch (start us, length us, event | category | flops | bytes accessed | tf_op | source)
XLA Modules:
  0.0 55.5 jit_solution(1614788264646056685)
XLA Ops:
  0.6 53.5 %shard_map.110 = (bf16[64,8,128]{2,1,0:T(8,128)(2,1)S(1)}, bf16[512,128]{1,0:T(8,128)(2,1)S(1)}, f32[8,128]{1,0:T(8,128)S(1)}, bf16[2048,128]{1,0:T(8,128)(2,1)S...) custom-call(bf16[128,2048]{1,0:T(8,128)(2,1)} %tok_hbm.1, bf16[128,2048]{1,0:T(8,128)(2,1)} %cot_hbm.1, ...), custom_call_target="tpu_custom_call" | custom-call | tf_op jit(solution)/shard_map/pallas_call | solution.py:564
  54.1 1.2 %shard_map.111 = (bf16[128,128]{1,0:T(8,128)(2,1)}, bf16[2,128]{1,0:T(2,128)(2,1)}, bf16[1,2048,128]{2,1,0:T(8,128)(2,1)}, bf16[1,2048,128]{2,1,0:T(8,128)(2,1)}, bf16[1,128,2048]{2,1,0:T(8,128)(2,1)}) custom-call(bf16[64,8,128]{2,1,0:T(8,128)(2,1)S(1)} %get-tuple-element.16.ret, bf16[512,128]{1,0:T(8,128)(2,1)S(1)} %get-tuple-element.17.p8, ...), custom_call_target="tpu_custom_call" | custom-call | tf_op jit(solution)/shard_map/pallas_call | solution.py:611

commit v6 on v3

--- a/solution.py
+++ b/solution.py
@@ -25,8 +25,14 @@
 WIDE = 2 * LANES
 QUADS = 4
 QUAD = 4 * LANES
-EARLY = "W r0 r1 r2 s3 A0 A1 t3 f0 f1 B0 f2 f3 H0 Q0 C0 A2 E0 A3 B1 Q1 H1 C1 H2 B2 Q2 C2 F0 H3 P3 B3 C3 E1 E3 E2 T G F1 F3 F2"
-LATE = "W r0 A0 r1 f0 f1 A1 r2 r3 B0 Q0 H0 C0 A2 H1 f2 E0 f3 B1 P1 C1 H3 B2 H2 A3 P2 C2 F0 E1 P3 E2 B3 F1 C3 F2 E3 F3 T G"
+EARLY = (
+    "W r0 r1 r2", "s3 A0 A1 t3", "f0 f1 B0 f2", "f3 H0 Q0 C0", "A2 E0 A3 B1",
+    "Q1 H1 C1 H2", "B2 Q2 C2 F0", "H3 P3 B3 C3", "E1 E3 E2 T", "G F1 F3 F2",
+)
+LATE = (
+    "W r0 A0 r1", "f0 f1 A1 r2", "r3 B0 Q0 H0", "C0 A2 H1 f2", "E0 f3 B1 P1",
+    "C1 H3 B2 H2", "A3 P2 C2 F0", "E1 P3 E2 B3", "F1 C3 F2 E3", "F3 T G",
+)
 
 
 def iota(shape, dim):
@@ -427,7 +433,7 @@
     steps = {"A": gather_out, "B": gather_in, "H": gather_far, "E": scatter_two, "F": give_back}
     def run(plan):
         left = {}
-        for step in plan.split():
+        for step in " ".join(plan).split():
             kind, g = step[0], int(step[1:] or 0)
             with jax.named_scope(step):
                 if kind == "r":

time: 58.6 us -> 58.6 us (level)
  no operation moved by 1% of the time
where the time goes in v6:
time: 58.6 us; the launch traced here: 58.2 us
  Pallas kernels  57.4 us (98%)
  between operations  0.82 us (1%)
    pallas_call x1, Pallas kernels, on_device(): pl.pallas_call(kernel, out_shape=(jax.ShapeDtypeStruct((nep, 8, LANES), B...  56.2 us
    pallas_call x1, Pallas kernels, on_device(): pl.pallas_call(finish, out_shape=(jax.ShapeDtypeStruct((tokn, LANES), BF)...  1.19 us

profile of v6, /device:TPU:1, one launch (start us, length us, event | category | flops | bytes accessed | tf_op | source)
XLA Modules:
  0.0 58.2 jit_solution(470533614580904353)
XLA Ops:
  0.6 56.2 %shard_map.110 = (bf16[64,8,128]{2,1,0:T(8,128)(2,1)S(1)}, bf16[512,128]{1,0:T(8,128)(2,1)S(1)}, f32[8,128]{1,0:T(8,128)S(1)}, bf16[2048,128]{1,0:T(8,128)(2,1)S...) custom-call(bf16[128,2048]{1,0:T(8,128)(2,1)} %tok_hbm.1, bf16[128,2048]{1,0:T(8,128)(2,1)} %cot_hbm.1, ...), custom_call_target="tpu_custom_call" | custom-call | tf_op jit(solution)/shard_map/pallas_call | solution.py:535
  56.8 1.2 %shard_map.111 = (bf16[128,128]{1,0:T(8,128)(2,1)}, bf16[2,128]{1,0:T(2,128)(2,1)}, bf16[1,2048,128]{2,1,0:T(8,128)(2,1)}, bf16[1,2048,128]{2,1,0:T(8,128)(2,1)}, bf16[1,128,2048]{2,1,0:T(8,128)(2,1)}) custom-call(bf16[64,8,128]{2,1,0:T(8,128)(2,1)S(1)} %get-tuple-element.16.ret, bf16[512,128]{1,0:T(8,128)(2,1)S(1)} %get-tuple-element.17.p8, ...), custom_call_target="tpu_custom_call" | custom-call | tf_op jit(solution)/shard_map/pallas_call | solution.py:581

commit v7 on v5

--- a/solution.py
+++ b/solution.py
@@ -32,8 +32,7 @@
 )
 LATE = (
     "W r0 A0 r1", "f0 f1 a1 r2", "r3 B0 z1 Q0", "H0 C0 B1 H1", "P1 C1 A2 f2",
-    "f3 E0 A3 E1", "y0 H2 B2 P2", "x0 C2 H3 P3", "F1 B3 C3 E2", "E3 F2 F3 T",
-    "G",
+    "f3 E0 A3 E1", "F0 H2 B2 P2", "C2 H3 P3 F1", "B3 C3 E2 E3", "F2 F3 T G",
 )
 
 

time: 55.6 us -> 55.7 us (level)
  no operation moved by 1% of the time
where the time goes in v7:
time: 55.7 us; the launch traced here: 55.5 us
  Pallas kernels  54.6 us (98%)
  between operations  0.82 us (1%)
    pallas_call x1, Pallas kernels, on_device(): pl.pallas_call(kernel, out_shape=(jax.ShapeDtypeStruct((nep, 8, LANES), B...  53.5 us
    pallas_call x1, Pallas kernels, on_device(): pl.pallas_call(finish, out_shape=(jax.ShapeDtypeStruct((tokn, LANES), BF)...  1.19 us

profile of v7, /device:TPU:1, one launch (start us, length us, event | category | flops | bytes accessed | tf_op | source)
XLA Modules:
  0.0 55.5 jit_solution(17675019146692231601)
XLA Ops:
  0.6 53.5 %shard_map.110 = (bf16[64,8,128]{2,1,0:T(8,128)(2,1)S(1)}, bf16[512,128]{1,0:T(8,128)(2,1)S(1)}, f32[8,128]{1,0:T(8,128)S(1)}, bf16[2048,128]{1,0:T(8,128)(2,1)S...) custom-call(bf16[128,2048]{1,0:T(8,128)(2,1)} %tok_hbm.1, bf16[128,2048]{1,0:T(8,128)(2,1)} %cot_hbm.1, ...), custom_call_target="tpu_custom_call" | custom-call | tf_op jit(solution)/shard_map/pallas_call | solution.py:563
  54.1 1.2 %shard_map.111 = (bf16[128,128]{1,0:T(8,128)(2,1)}, bf16[2,128]{1,0:T(2,128)(2,1)}, bf16[1,2048,128]{2,1,0:T(8,128)(2,1)}, bf16[1,2048,128]{2,1,0:T(8,128)(2,1)}, bf16[1,128,2048]{2,1,0:T(8,128)(2,1)}) custom-call(bf16[64,8,128]{2,1,0:T(8,128)(2,1)S(1)} %get-tuple-element.16.ret, bf16[512,128]{1,0:T(8,128)(2,1)S(1)} %get-tuple-element.17.p8, ...), custom_call_target="tpu_custom_call" | custom-call | tf_op jit(solution)/shard_map/pallas_call | solution.py:610
